TPU v7x, 32 devices: a whole 2x2x4 slice. The times are simulated.
32 devices in a mesh: ep: 8 (over z, x), tp: 4 (over y, core).
Axes of the slice: x: 2, y: 2, z: 4, core: 2. Of those that a mesh axis runs over, the one named last changes fastest.
Arguments:
- tokens: bfloat16 [4096, 2048], P(('ep', 'tp')), may hold values from -6 to 6
- expert_ids: int32 [4096, 4], P(('ep', 'tp')), may hold values from 0 to 7, all different within a row; in each aligned block of 128 rows (0 to 127, 128 to 255, ...) at most 96 rows name the same one
- route_weights: float32 [4096, 4], P(('ep', 'tp')), may hold values from 0.2 to 1.2
- cotangent: bfloat16 [4096, 2048], P(('ep', 'tp')), may hold values from -6 to 6
- gate_weight: bfloat16 [32, 512, 2048], P(('ep', 'tp')), may hold values from -0.125 to 0.125
- up_weight: bfloat16 [32, 512, 2048], P(('ep', 'tp')), may hold values from -0.125 to 0.125
- down_weight: bfloat16 [32, 512, 2048], P(('ep', 'tp')), may hold values from -0.25 to 0.25
- shared_gate: bfloat16 [256, 2048], replicated, may hold values from -0.125 to 0.125
- shared_up: bfloat16 [256, 2048], replicated, may hold values from -0.125 to 0.125
- shared_down: bfloat16 [256, 2048], replicated, may hold values from -0.375 to 0.375
Outputs:
- token_grad: bfloat16 [4096, 2048], P(('ep', 'tp'))
- route_grad: float32 [4096, 4], P(('ep', 'tp'))
- gate_grad: bfloat16 [32, 512, 2048], P(('ep', 'tp'))
- up_grad: bfloat16 [32, 512, 2048], P(('ep', 'tp'))
- down_grad: bfloat16 [32, 512, 2048], P(('ep', 'tp'))
- shared_grads: float32 [2048, 3, 256], P(('ep', 'tp'))
Inputs may be any that keep to these rules, and one draw needn't show every extreme that they name: `expert_ids`: each row names 4 different numbers of 0 to 7, experts within the group of the row's device. Among the rows of one device (aligned blocks of 128 tokens) no number is named more than 96 times, and in some blocks one number is named exactly 96 times.
All inputs are finite; a program needn't handle non-finite values.
Results may differ from a plain program's by a relative error of at most 0.006.
Values may be sent and summed in bfloat16 or wider, within the bound.
A program may use at most 128 MiB of HBM per device.

v0:
```python
import functools

import jax
import jax.numpy as jnp
from jax import lax
from jax.experimental import pallas as pl
from jax.experimental.pallas import tpu as pltpu
from jax.sharding import PartitionSpec as P


def gated_backward(scaled, gate_pre, up_pre):
    sigmoid_gate = jax.nn.sigmoid(gate_pre)
    gate_delta = (scaled * up_pre * sigmoid_gate * (1.0 + gate_pre * (1.0 - sigmoid_gate))).astype(
        jnp.bfloat16
    )
    up_delta = (scaled * jax.nn.silu(gate_pre)).astype(jnp.bfloat16)
    return (gate_delta, up_delta)


def forward_products(token_rows, gate_local, up_local):
    gate_pre = jnp.einsum("rd,fd->rf", token_rows, gate_local, preferred_element_type=jnp.float32)
    up_pre = jnp.einsum("rd,fd->rf", token_rows, up_local, preferred_element_type=jnp.float32)
    return (gate_pre, up_pre)


def exchanged_shards(
    tokens,
    expert_ids,
    route_weights,
    cotangent,
    gate_weight,
    up_weight,
    down_weight,
    shared_gate,
    shared_up,
    shared_down,
):
    ep_size = lax.axis_size("ep")
    tok_rows = tokens.shape[0]
    model_width = tokens.shape[1]
    top_count = expert_ids.shape[1]
    capacity = 3 * tok_rows * top_count // (2 * ep_size)
    slots_all = ep_size * capacity
    assign_count = tok_rows * top_count
    flat_ids = expert_ids.reshape(-1)
    one_hot = (flat_ids[:, None] == jnp.arange(ep_size, dtype=jnp.int32)[None, :]).astype(jnp.int32)
    slot_index = jnp.sum(jnp.cumsum(one_hot, axis=0) * one_hot, axis=1) - 1
    position = flat_ids * capacity + slot_index
    row_assign = (
        jnp.full((slots_all,), assign_count, jnp.int32)
        .at[position]
        .set(jnp.arange(assign_count, dtype=jnp.int32))
    )
    row_token = row_assign // top_count
    row_weight = jnp.take(
        jnp.concatenate([route_weights.reshape(-1), jnp.zeros((1,), jnp.float32)], axis=0),
        row_assign,
        axis=0,
    )
    empty_row = jnp.zeros((1, model_width), jnp.bfloat16)
    send_tokens = jnp.take(jnp.concatenate([tokens, empty_row], axis=0), row_token, axis=0).reshape(
        ep_size, capacity, model_width
    )
    send_cot = jnp.take(jnp.concatenate([cotangent, empty_row], axis=0), row_token, axis=0).reshape(
        ep_size, capacity, model_width
    )
    gate_local = gate_weight[0]
    up_local = up_weight[0]
    down_local = down_weight[0]
    scales = lax.all_to_all(
        row_weight.reshape(ep_size, capacity), "ep", split_axis=0, concat_axis=0, tiled=True
    ).reshape(slots_all)
    token_rows, cot_rows = (
        lax.all_to_all(send_tokens, "ep", split_axis=0, concat_axis=0, tiled=True),
        lax.all_to_all(send_cot, "ep", split_axis=0, concat_axis=0, tiled=True),
    )
    token_rows = token_rows.reshape(slots_all, model_width)
    cot_rows = cot_rows.reshape(slots_all, model_width)
    gate_pre, up_pre = forward_products(token_rows, gate_local, up_local)
    hidden = (jax.nn.silu(gate_pre) * up_pre).astype(jnp.bfloat16)
    back_hidden = jnp.einsum("rd,fd->rf", cot_rows, down_local, preferred_element_type=jnp.float32)
    route_part = jnp.sum(back_hidden * hidden.astype(jnp.float32), axis=1)
    gate_delta, up_delta = gated_backward(scales[:, None] * back_hidden, gate_pre, up_pre)
    weighted_cot = (scales[:, None] * cot_rows.astype(jnp.float32)).astype(jnp.bfloat16)
    token_part = jnp.einsum(
        "rf,fd->rd", gate_delta, gate_local, preferred_element_type=jnp.float32
    ) + jnp.einsum("rf,fd->rd", up_delta, up_local, preferred_element_type=jnp.float32)
    gate_grad = jnp.einsum(
        "rf,rd->fd", gate_delta, token_rows, preferred_element_type=jnp.float32
    ).astype(jnp.bfloat16)[None]
    up_grad = jnp.einsum(
        "rf,rd->fd", up_delta, token_rows, preferred_element_type=jnp.float32
    ).astype(jnp.bfloat16)[None]
    down_grad = jnp.einsum(
        "rf,rd->fd", hidden, weighted_cot, preferred_element_type=jnp.float32
    ).astype(jnp.bfloat16)[None]
    back_rows, back_route = (
        lax.all_to_all(
            token_part.reshape(ep_size, capacity, model_width),
            "ep",
            split_axis=0,
            concat_axis=0,
            tiled=True,
        ),
        lax.all_to_all(
            route_part.reshape(ep_size, capacity), "ep", split_axis=0, concat_axis=0, tiled=True
        ),
    )
    routed = jnp.sum(
        jnp.take(back_rows.reshape(slots_all, model_width), position, axis=0).reshape(
            tok_rows, top_count, model_width
        ),
        axis=1,
    )
    route_grad = jnp.take(back_route.reshape(slots_all), position, axis=0).reshape(
        tok_rows, top_count
    )
    common_gate = jnp.einsum("td,fd->tf", tokens, shared_gate, preferred_element_type=jnp.float32)
    common_up = jnp.einsum("td,fd->tf", tokens, shared_up, preferred_element_type=jnp.float32)
    common_hidden = (jax.nn.silu(common_gate) * common_up).astype(jnp.bfloat16)
    common_back = jnp.einsum(
        "td,fd->tf", cotangent, shared_down, preferred_element_type=jnp.float32
    )
    common_gate_delta, common_up_delta = gated_backward(common_back, common_gate, common_up)
    common_part = jnp.einsum(
        "tf,fd->td", common_gate_delta, shared_gate, preferred_element_type=jnp.float32
    ) + jnp.einsum("tf,fd->td", common_up_delta, shared_up, preferred_element_type=jnp.float32)
    shared_grads = lax.psum_scatter(
        jnp.stack(
            [
                jnp.einsum(
                    "tc,tf->cf", tokens, common_gate_delta, preferred_element_type=jnp.float32
                ),
                jnp.einsum(
                    "tc,tf->cf", tokens, common_up_delta, preferred_element_type=jnp.float32
                ),
                jnp.einsum(
                    "tc,tf->cf", cotangent, common_hidden, preferred_element_type=jnp.float32
                ),
            ],
            axis=1,
        ),
        ("ep", "tp"),
        scatter_dimension=0,
        tiled=True,
    )
    token_grad = (routed + common_part).astype(jnp.bfloat16)
    return (token_grad, route_grad, gate_grad, up_grad, down_grad, shared_grads)


MESH = pl.DeviceIdType.MESH


def ring_place(index, count):
    odd = lax.rem(index, 2)
    pair = lax.div(index, 2)
    return (1 - odd) * pair + odd * (count - 1 - pair)


def ring_index(place, count):
    place = lax.rem(place + 2 * count, count)
    late = lax.div(place, (count + 1) // 2)
    return (1 - late) * (2 * place) + late * (2 * (count - 1 - place) + 1)


def greet(groups):
    barrier = pltpu.get_barrier_semaphore()
    total = 0
    for axis, count in groups:
        me = lax.axis_index(axis)
        for step in range(1, count):
            pl.semaphore_signal(
                barrier,
                inc=1,
                device_id={axis: lax.rem(me + step, count)},
                device_id_type=MESH,
            )
            total += 1
    pl.semaphore_wait(barrier, total)


def remote(src, dst, send_sem, recv_sem, axis, index):
    return pltpu.make_async_remote_copy(
        src_ref=src,
        dst_ref=dst,
        send_sem=send_sem,
        recv_sem=recv_sem,
        device_id={axis: index},
        device_id_type=MESH,
    )


def spread_rows(src, dst, send_sem, recv_sem, axis, count):
    me = lax.axis_index(axis)
    copies = []
    for step in range(1, count):
        peer = lax.rem(me + step, count)
        copies.append(
            remote(src.at[peer], dst.at[me], send_sem.at[step - 1], recv_sem.at[step - 1], axis, peer)
        )
    return copies


def dot_nt(left, right):
    return lax.dot_general(
        left, right, (((1,), (1,)), ((), ())), preferred_element_type=jnp.float32
    )


def deltas(scaled, gate_pre, up_pre):
    sigmoid_gate = jax.nn.sigmoid(gate_pre)
    silu_gate = gate_pre * sigmoid_gate
    gate_delta = scaled * up_pre * sigmoid_gate * (1.0 + gate_pre * (1.0 - sigmoid_gate))
    return gate_delta, scaled * silu_gate, silu_gate * up_pre


def layer_kernel(
    count,
    group,
    tok,
    cot,
    wts,
    gate_w,
    up_w,
    down_w,
    shared_gate,
    shared_up,
    shared_down,
    token_out,
    route_out,
    gate_out,
    up_out,
    down_out,
    shared_out,
    all_tok,
    all_cot,
    all_wts,
    tok_w,
    cot_w,
    pre,
    turned,
    shared_turned,
    part,
    own_part,
    held,
    outgoing,
    route_buf,
    shared_part,
    shared_send,
    shared_in,
    stage,
    total_grad,
    gsend,
    grecv,
    rsend,
    rrecv,
    load_sem,
    wsend,
    wrecv,
    bsend,
    brecv,
    ssend,
    srecv,
    own_sem,
    out_sem,
):
    me = lax.axis_index("ep")
    mine = lax.axis_index("tp")
    place = ring_place(me, count)
    rows, width = tok.shape
    half = rows // 2
    hid = gate_w.shape[0]
    common = shared_gate.shape[0]
    sides = (ring_index(place + 1, count), ring_index(place - 1, count))
    halves = (pl.ds(0, half), pl.ds(half, half))

    loads = [
        pltpu.make_async_copy(src, dst, load_sem.at[i])
        for i, (src, dst) in enumerate(
            (
                (tok, all_tok.at[0]),
                (cot, all_cot.at[0]),
                (gate_w, tok_w.at[pl.ds(0, hid)]),
                (up_w, tok_w.at[pl.ds(hid, hid)]),
                (shared_gate, tok_w.at[pl.ds(2 * hid, common)]),
                (shared_up, tok_w.at[pl.ds(2 * hid + common, common)]),
                (down_w, cot_w.at[pl.ds(0, hid)]),
                (shared_down, cot_w.at[pl.ds(hid, common)]),
            )
        )
    ]
    for copy in loads:
        copy.start()
    greet((("ep", count), ("tp", group)))

    def passed(step, array, side):
        slots = (all_tok, all_cot)[array]
        return remote(
            slots.at[step, halves[side]],
            slots.at[step + 1, halves[side]],
            gsend.at[array, side, step],
            grecv.at[array, side, step],
            "ep",
            sides[side],
        )

    def hop(step, side):
        return remote(
            outgoing.at[step - 1, halves[side]],
            held.at[step - 1, halves[side]],
            rsend.at[side, step - 1],
            rrecv.at[side, step - 1],
            "ep",
            sides[side],
        )

    loads[0].wait()
    passed(0, 0, 0).start()
    passed(0, 0, 1).start()
    loads[1].wait()
    passed(0, 1, 0).start()
    passed(0, 1, 1).start()
    weights = spread_rows(wts, all_wts, wsend, wrecv, "ep", count)
    for copy in weights:
        copy.start()
    own_weights = pltpu.make_async_copy(wts.at[me], all_wts.at[me], own_sem.at[0])
    own_weights.start()
    route_buf[...] = jnp.zeros_like(route_buf)
    for copy in loads[2:]:
        copy.wait()
    for copy in weights:
        copy.wait()
    own_weights.wait()

    early = [count - 3 + i for i in range(3)]
    tile = width // count

    def add_tiles(i, start, end, last):
        slots = all_cot if i == 2 else all_tok

        def tile_body(j, carry):
            cols = pl.ds(pl.multiple_of(j * tile, tile), tile)
            block = slots[pl.ds(start, end - start), :, cols].reshape((end - start) * rows, tile)
            left = turned[i, :, pl.ds(start * rows, (end - start) * rows)]
            grad = jnp.dot(left, block, preferred_element_type=jnp.float32)
            if last:
                stage[i, :, cols] = (total_grad[i, :, cols] + grad).astype(jnp.bfloat16)
            else:
                total_grad[i, :, cols] = grad
            return carry

        lax.fori_loop(0, count, tile_body, 0)

    def body(step, carry):
        def pass_on(array):
            @pl.when(step > 0)
            def _():
                for side in (0, 1):
                    passed(step - 1, array, side).wait_recv()

                    @pl.when(step < count - 1)
                    def _():
                        passed(step, array, side).start()

        pass_on(0)
        first = ring_index(place - step, count)
        second = ring_index(place + step, count)
        lane = lax.broadcasted_iota(jnp.int32, (1, rows), 1)
        eye = lax.broadcasted_iota(jnp.int32, (rows, rows), 0) == lax.broadcasted_iota(
            jnp.int32, (rows, rows), 1
        )
        scale_row = jnp.where(lane < half, all_wts[first], all_wts[second])
        scale = jnp.sum(jnp.where(eye, scale_row, 0.0), axis=1, keepdims=True)

        pre[...] = dot_nt(all_tok[step], tok_w[...])
        pass_on(1)
        back_hidden = dot_nt(all_cot[step], cot_w[pl.ds(0, hid)])
        gate_pre, up_pre = pre[:, pl.ds(0, hid)], pre[:, pl.ds(hid, hid)]
        gate_delta, up_delta, hidden = deltas(scale * back_hidden, gate_pre, up_pre)
        both = jnp.concatenate([gate_delta, up_delta], axis=1).astype(jnp.bfloat16)
        part[...] = jnp.dot(both, tok_w[pl.ds(0, 2 * hid)], preferred_element_type=jnp.float32)

        @pl.when(step == 1)
        def _():
            outgoing[0] = part[...].astype(jnp.bfloat16)
            for side in (0, 1):
                hop(step, side).start()

        @pl.when(step > 1)
        def _():
            for side in (0, 1):
                hop(step - 1, side).wait_recv()
                outgoing[step - 1, halves[side]] = (
                    held[step - 2, halves[side]].astype(jnp.float32) + part[halves[side]]
                ).astype(jnp.bfloat16)
                hop(step, side).start()

        rounded = hidden.astype(jnp.bfloat16).astype(jnp.float32)
        route = jnp.sum(back_hidden * rounded, axis=1, keepdims=True)
        route_row = jnp.sum(jnp.where(eye, route, 0.0), axis=0, keepdims=True)
        route_buf[first] = jnp.where(lane < half, route_row, route_buf[first])
        route_buf[second] = jnp.where(lane < half, route_buf[second], route_row)
        columns = pl.ds(pl.multiple_of(step * rows, rows), rows)
        turned[0, :, columns] = gate_delta.T.astype(jnp.bfloat16)
        turned[1, :, columns] = up_delta.T.astype(jnp.bfloat16)
        turned[2, :, columns] = (scale * hidden).T.astype(jnp.bfloat16)

        common_back = dot_nt(all_cot[step], cot_w[pl.ds(hid, common)])
        common_gate = pre[:, pl.ds(2 * hid, common)]
        common_up = pre[:, pl.ds(2 * hid + common, common)]
        common_deltas = deltas(common_back, common_gate, common_up)
        for i in range(3):
            shared_turned[i, :, columns] = common_deltas[i].T.astype(jnp.bfloat16)

        @pl.when(step == 0)
        def _():
            pair = jnp.concatenate(common_deltas[:2], axis=1).astype(jnp.bfloat16)
            own_part[...] = part[...] + jnp.dot(
                pair, tok_w[pl.ds(2 * hid, 2 * common)], preferred_element_type=jnp.float32
            )

        for i in range(3):

            @pl.when(step == count - 4 + i)
            def _():
                add_tiles(i, 0, early[i], False)

        return carry

    lax.fori_loop(0, count, body, 0)

    span = width // count
    piece = span // group
    mine_cols = pl.ds(pl.multiple_of(me * span, span), span)
    for i, slots in enumerate((all_tok, all_tok, all_cot)):
        block = slots[:, :, mine_cols].reshape(count * rows, span)
        grad = jnp.dot(shared_turned[i], block, preferred_element_type=jnp.float32).T
        for peer in range(group):
            shared_part[peer, i] = grad[peer * piece : (peer + 1) * piece]
            shared_send[peer, i] = grad[peer * piece : (peer + 1) * piece].astype(jnp.bfloat16)
    small = spread_rows(route_buf, route_out, bsend, brecv, "ep", count)
    small += spread_rows(shared_send, shared_in, ssend, srecv, "tp", group)
    for copy in small:
        copy.start()
    own_route = pltpu.make_async_copy(route_buf.at[me], route_out.at[me], own_sem.at[1])
    own_route.start()

    writes = []
    for i, out in enumerate((gate_out, up_out, down_out)):
        add_tiles(i, early[i], count, True)
        writes.append(pltpu.make_async_copy(stage.at[i], out, out_sem.at[i]))
        writes[-1].start()

    for side in (0, 1):
        hop(count - 1, side).wait_recv()
        token_out[halves[side]] = (
            held[count - 2, halves[side]].astype(jnp.float32) + own_part[halves[side]]
        ).astype(jnp.bfloat16)
    for copy in small:
        copy.wait()
    own_route.wait()
    total = shared_part[mine]
    for step in range(1, group):
        total = total + shared_in[lax.rem(mine + step, group)].astype(jnp.float32)
    shared_out[...] = total
    for step in range(count - 1):
        for side in (0, 1):
            for array in (0, 1):
                passed(step, array, side).wait_send()
            hop(step + 1, side).wait_send()
    for copy in writes:
        copy.wait()


def layer(tokens, cotangent, dense_weights, experts, commons, count, group):
    rows, width = tokens.shape
    hid, common = experts[0].shape[0], commons[0].shape[0]
    piece = width // count // group
    vmem = pl.BlockSpec(memory_space=pltpu.VMEM)
    anywhere = pl.BlockSpec(memory_space=pl.ANY)
    grad = jax.ShapeDtypeStruct((hid, width), jnp.bfloat16)
    shared = (3, piece, common)
    return pl.pallas_call(
        functools.partial(layer_kernel, count, group),
        out_shape=(
            jax.ShapeDtypeStruct((rows, width), jnp.bfloat16),
            jax.ShapeDtypeStruct((count, 1, rows), jnp.float32),
            grad,
            grad,
            grad,
            jax.ShapeDtypeStruct(shared, jnp.float32),
        ),
        in_specs=[anywhere, anywhere, vmem] + [anywhere] * 6,
        out_specs=(vmem, vmem, anywhere, anywhere, anywhere, vmem),
        scratch_shapes=[
            pltpu.VMEM((count, rows, width), jnp.bfloat16),
            pltpu.VMEM((count, rows, width), jnp.bfloat16),
            pltpu.VMEM((count, 1, rows), jnp.float32),
            pltpu.VMEM((2 * hid + 2 * common, width), jnp.bfloat16),
            pltpu.VMEM((hid + common, width), jnp.bfloat16),
            pltpu.VMEM((rows, 2 * hid + 2 * common), jnp.float32),
            pltpu.VMEM((3, hid, count * rows), jnp.bfloat16),
            pltpu.VMEM((3, common, count * rows), jnp.bfloat16),
            pltpu.VMEM((rows, width), jnp.float32),
            pltpu.VMEM((rows, width), jnp.float32),
            pltpu.VMEM((count - 1, rows, width), jnp.bfloat16),
            pltpu.VMEM((count - 1, rows, width), jnp.bfloat16),
            pltpu.VMEM((count, 1, rows), jnp.float32),
            pltpu.VMEM((group,) + shared, jnp.float32),
            pltpu.VMEM((group,) + shared, jnp.bfloat16),
            pltpu.VMEM((group,) + shared, jnp.bfloat16),
            pltpu.VMEM((3, hid, width), jnp.bfloat16),
            pltpu.VMEM((3, hid, width), jnp.float32),
            pltpu.SemaphoreType.DMA((2, 2, count - 1)),
            pltpu.SemaphoreType.DMA((2, 2, count - 1)),
            pltpu.SemaphoreType.DMA((2, count - 1)),
            pltpu.SemaphoreType.DMA((2, count - 1)),
            pltpu.SemaphoreType.DMA((8,)),
            pltpu.SemaphoreType.DMA((count - 1,)),
            pltpu.SemaphoreType.DMA((count - 1,)),
            pltpu.SemaphoreType.DMA((count - 1,)),
            pltpu.SemaphoreType.DMA((count - 1,)),
            pltpu.SemaphoreType.DMA((group - 1,)),
            pltpu.SemaphoreType.DMA((group - 1,)),
            pltpu.SemaphoreType.DMA((2,)),
            pltpu.SemaphoreType.DMA((3,)),
        ],
        compiler_params=pltpu.CompilerParams(collective_id=0, has_side_effects=True),
    )(tokens, cotangent, dense_weights, *experts, *commons)


def gathered_shards(
    tokens,
    expert_ids,
    route_weights,
    cotangent,
    gate_weight,
    up_weight,
    down_weight,
    shared_gate,
    shared_up,
    shared_down,
):
    count, group = lax.axis_size("ep"), lax.axis_size("tp")
    rows = tokens.shape[0]
    chosen = expert_ids[None, :, :] == jnp.arange(count, dtype=jnp.int32)[:, None, None]
    dense_weights = jnp.sum(jnp.where(chosen, route_weights[None], 0.0), axis=2)[:, None, :]
    token_grad, back_route, gate_grad, up_grad, down_grad, shared_sum = layer(
        tokens,
        cotangent,
        dense_weights,
        (gate_weight[0], up_weight[0], down_weight[0]),
        (shared_gate, shared_up, shared_down),
        count,
        group,
    )
    route_grad = jnp.sum(jnp.where(chosen, back_route.reshape(count, rows, 1), 0.0), axis=0)
    return (
        token_grad,
        route_grad,
        gate_grad[None],
        up_grad[None],
        down_grad[None],
        jnp.transpose(shared_sum, (1, 0, 2)),
    )


def shards(tokens, expert_ids, *rest):
    dense = 4 <= lax.axis_size("ep") <= 2 * expert_ids.shape[1]
    return (gathered_shards if dense else exchanged_shards)(tokens, expert_ids, *rest)


def solution(mesh):
    in_specs = (
        P(("ep", "tp"), None),
        P(("ep", "tp"), None),
        P(("ep", "tp"), None),
        P(("ep", "tp"), None),
        P(("ep", "tp"), None, None),
        P(("ep", "tp"), None, None),
        P(("ep", "tp"), None, None),
        P(),
        P(),
        P(),
    )
    out_specs = (
        P(("ep", "tp"), None),
        P(("ep", "tp"), None),
        P(("ep", "tp"), None, None),
        P(("ep", "tp"), None, None),
        P(("ep", "tp"), None, None),
        P(("ep", "tp"), None, None),
    )
    return jax.shard_map(shards, mesh=mesh, in_specs=in_specs, out_specs=out_specs, check_vma=False)
```

profile of v0, /device:TPU:0, one launch (start us, length us, event | category | flops | bytes accessed | tf_op | source)
XLA Modules:
  0.0 151.6 jit_solution(9360104031982154365)
XLA Ops:
  0.6 1.3 select_reduce_fusion.1
  1.9 0.0 copy-start.3
  1.9 138.8 %shard_map.145 = (bf16[128,2048]{1,0:T(8,128)(2,1)}, f32[8,1,128]{2,1,0:T(1,128)}, bf16[512,2048]{1,0:T(8,128)(2,1)}, bf16[512,2048]{1,0:T(8,128)(2,1)}, bf16[51...) custom-call(bf16[128,2048]{1,0:T(8,128)(2,1)} %tok.1, bf16[128,2048]{1,0:T(8,128)(2,1)} %cot.1, f32[8,1,128]{2,1,0:T(1,128)} %bitcast.16, ...), custom_call_target="tpu_custom_call" | custom-call | tf_op jit(solution)/shard_map/pallas_call | solution.py:483
  140.8 0.0 copy-done.3
  140.8 1.3 select_reduce_fusion
  142.1 1.9 %copy.23 = bf16[128,2048]{1,0:T(8,128)(2,1)} copy(bf16[128,2048]{1,0:T(8,128)(2,1)} %get-tuple-element.24) | data formatting | bytes 1048576
  144.0 0.0 copy-start.1
  144.0 3.3 %copy.24 = bf16[1,512,2048]{2,1,0:T(8,128)(2,1)} copy(bf16[1,512,2048]{2,1,0:T(8,128)(2,1)} %bitcast.14) | data formatting | bytes 4194304
  147.3 0.0 copy-done.1
  147.3 0.0 copy-start
  147.3 1.3 copy.25
  148.6 1.0 copy-done
  149.6 0.0 copy-start.2
  149.6 1.3 copy.26
  150.9 0.0 copy-done.2
  150.9 0.7 copy.27
Async XLA Ops:
  1.9 138.9 %copy-start.3 = (s32[128,4]{0,1:T(4,128)S(1)}, s32[128,4]{0,1:T(4,128)}, u32[]{:S(2)}) copy-start(s32[128,4]{0,1:T(4,128)} %param.11) | copy-start | bytes 6148
  144.0 3.3 %copy-start.1 = (bf16[512,2048]{1,0:T(8,128)(2,1)S(1)}, bf16[512,2048]{1,0:T(8,128)(2,1)}, u32[]{:S(2)}) copy-start(bf16[512,2048]{1,0:T(8,128)(2,1)} %get-tuple-element.15) | copy-start | bytes 6291460
  147.3 2.3 %copy-start = (bf16[512,2048]{1,0:T(8,128)(2,1)S(1)}, bf16[512,2048]{1,0:T(8,128)(2,1)}, u32[]{:S(2)}) copy-start(bf16[512,2048]{1,0:T(8,128)(2,1)} %get-tuple-element.16) | copy-start | bytes 6291460
  149.6 1.3 copy-start.2
where the time goes:
time: 152 us
  Pallas kernels  139 us (91%)
  local copies, waits for them, and re-layouts  9.54 us (6%)
  other arithmetic  2.58 us (2%)
    pallas_call x1, Pallas kernels, layer(): pl.pallas_call(functools.partial(layer_kernel, count, group), out_shape=(...  139 us
    unnamed x13, local copies, waits for them, and re-layouts  9.54 us

commit v1 on v0

--- a/solution.py
+++ b/solution.py
@@ -219,7 +219,8 @@
     group,
     tok,
     cot,
-    wts,
+    ids,
+    chosen_w,
     gate_w,
     up_w,
     down_w,
@@ -232,6 +233,8 @@
     up_out,
     down_out,
     shared_out,
+    wts,
+    route_in,
     all_tok,
     all_cot,
     all_wts,
@@ -248,7 +251,6 @@
     shared_part,
     shared_send,
     shared_in,
-    stage,
     total_grad,
     gsend,
     grecv,
@@ -262,7 +264,6 @@
     ssend,
     srecv,
     own_sem,
-    out_sem,
 ):
     me = lax.axis_index("ep")
     mine = lax.axis_index("tp")
@@ -291,6 +292,10 @@
     ]
     for copy in loads:
         copy.start()
+    for expert in range(count):
+        wts[expert] = jnp.sum(
+            jnp.where(ids[...] == expert, chosen_w[...], 0.0), axis=0, keepdims=True
+        )
     greet((("ep", count), ("tp", group)))
 
     def passed(step, array, side):
@@ -332,6 +337,7 @@
         copy.wait()
     own_weights.wait()
 
+    outs = (gate_out, up_out, down_out)
     early = [count - 3 + i for i in range(3)]
     tile = width // count
 
@@ -344,7 +350,7 @@
             left = turned[i, :, pl.ds(start * rows, (end - start) * rows)]
             grad = jnp.dot(left, block, preferred_element_type=jnp.float32)
             if last:
-                stage[i, :, cols] = (total_grad[i, :, cols] + grad).astype(jnp.bfloat16)
+                outs[i][:, cols] = (total_grad[i, :, cols] + grad).astype(jnp.bfloat16)
             else:
                 total_grad[i, :, cols] = grad
             return carry
@@ -438,18 +444,15 @@
         for peer in range(group):
             shared_part[peer, i] = grad[peer * piece : (peer + 1) * piece]
             shared_send[peer, i] = grad[peer * piece : (peer + 1) * piece].astype(jnp.bfloat16)
-    small = spread_rows(route_buf, route_out, bsend, brecv, "ep", count)
+    small = spread_rows(route_buf, route_in, bsend, brecv, "ep", count)
     small += spread_rows(shared_send, shared_in, ssend, srecv, "tp", group)
     for copy in small:
         copy.start()
-    own_route = pltpu.make_async_copy(route_buf.at[me], route_out.at[me], own_sem.at[1])
+    own_route = pltpu.make_async_copy(route_buf.at[me], route_in.at[me], own_sem.at[1])
     own_route.start()
 
-    writes = []
-    for i, out in enumerate((gate_out, up_out, down_out)):
+    for i in range(3):
         add_tiles(i, early[i], count, True)
-        writes.append(pltpu.make_async_copy(stage.at[i], out, out_sem.at[i]))
-        writes[-1].start()
 
     for side in (0, 1):
         hop(count - 1, side).wait_recv()
@@ -459,6 +462,10 @@
     for copy in small:
         copy.wait()
     own_route.wait()
+    routes = jnp.zeros(ids.shape, jnp.float32)
+    for expert in range(count):
+        routes = jnp.where(ids[...] == expert, route_in[expert], routes)
+    route_out[...] = routes
     total = shared_part[mine]
     for step in range(1, group):
         total = total + shared_in[lax.rem(mine + step, group)].astype(jnp.float32)
@@ -468,31 +475,31 @@
             for array in (0, 1):
                 passed(step, array, side).wait_send()
             hop(step + 1, side).wait_send()
-    for copy in writes:
-        copy.wait()
-
-
-def layer(tokens, cotangent, dense_weights, experts, commons, count, group):
+
+
+def layer(tokens, cotangent, ids, weights, experts, commons, count, group):
     rows, width = tokens.shape
     hid, common = experts[0].shape[0], commons[0].shape[0]
     piece = width // count // group
     vmem = pl.BlockSpec(memory_space=pltpu.VMEM)
     anywhere = pl.BlockSpec(memory_space=pl.ANY)
-    grad = jax.ShapeDtypeStruct((hid, width), jnp.bfloat16)
+    grad = pltpu.VMEM((hid, width), jnp.bfloat16)
     shared = (3, piece, common)
     return pl.pallas_call(
         functools.partial(layer_kernel, count, group),
         out_shape=(
-            jax.ShapeDtypeStruct((rows, width), jnp.bfloat16),
-            jax.ShapeDtypeStruct((count, 1, rows), jnp.float32),
+            pltpu.VMEM((rows, width), jnp.bfloat16),
+            pltpu.VMEM(ids.shape, jnp.float32),
             grad,
             grad,
             grad,
-            jax.ShapeDtypeStruct(shared, jnp.float32),
+            pltpu.VMEM(shared, jnp.float32),
         ),
-        in_specs=[anywhere, anywhere, vmem] + [anywhere] * 6,
-        out_specs=(vmem, vmem, anywhere, anywhere, anywhere, vmem),
+        in_specs=[anywhere, anywhere, vmem, vmem] + [anywhere] * 6,
+        out_specs=(vmem,) * 6,
         scratch_shapes=[
+            pltpu.VMEM((count, 1, rows), jnp.float32),
+            pltpu.VMEM((count, 1, rows), jnp.float32),
             pltpu.VMEM((count, rows, width), jnp.bfloat16),
             pltpu.VMEM((count, rows, width), jnp.bfloat16),
             pltpu.VMEM((count, 1, rows), jnp.float32),
@@ -509,7 +516,6 @@
             pltpu.VMEM((group,) + shared, jnp.float32),
             pltpu.VMEM((group,) + shared, jnp.bfloat16),
             pltpu.VMEM((group,) + shared, jnp.bfloat16),
-            pltpu.VMEM((3, hid, width), jnp.bfloat16),
             pltpu.VMEM((3, hid, width), jnp.float32),
             pltpu.SemaphoreType.DMA((2, 2, count - 1)),
             pltpu.SemaphoreType.DMA((2, 2, count - 1)),
@@ -523,10 +529,33 @@
             pltpu.SemaphoreType.DMA((group - 1,)),
             pltpu.SemaphoreType.DMA((group - 1,)),
             pltpu.SemaphoreType.DMA((2,)),
-            pltpu.SemaphoreType.DMA((3,)),
         ],
-        compiler_params=pltpu.CompilerParams(collective_id=0, has_side_effects=True),
-    )(tokens, cotangent, dense_weights, *experts, *commons)
+        compiler_params=pltpu.CompilerParams(
+            collective_id=0, has_side_effects=True, vmem_limit_bytes=53 * 2**20
+        ),
+    )(tokens, cotangent, ids, weights, *experts, *commons)
+
+
+def flush_kernel(count, *refs):
+    copies = [
+        pltpu.make_async_copy(refs[i], refs[count + i], refs[2 * count].at[i]) for i in range(count)
+    ]
+    for copy in copies:
+        copy.start()
+    for copy in copies:
+        copy.wait()
+
+
+def flush(*held):
+    count = len(held)
+    return pl.pallas_call(
+        functools.partial(flush_kernel, count),
+        out_shape=tuple(jax.ShapeDtypeStruct(x.shape, x.dtype) for x in held),
+        in_specs=[pl.BlockSpec(memory_space=pltpu.VMEM)] * count,
+        out_specs=(pl.BlockSpec(memory_space=pl.ANY),) * count,
+        scratch_shapes=[pltpu.SemaphoreType.DMA((count,))],
+        compiler_params=pltpu.CompilerParams(vmem_limit_bytes=2**20),
+    )(*held)
 
 
 def gathered_shards(
@@ -542,22 +571,20 @@
     shared_down,
 ):
     count, group = lax.axis_size("ep"), lax.axis_size("tp")
-    rows = tokens.shape[0]
-    chosen = expert_ids[None, :, :] == jnp.arange(count, dtype=jnp.int32)[:, None, None]
-    dense_weights = jnp.sum(jnp.where(chosen, route_weights[None], 0.0), axis=2)[:, None, :]
-    token_grad, back_route, gate_grad, up_grad, down_grad, shared_sum = layer(
+    held = layer(
         tokens,
         cotangent,
-        dense_weights,
+        expert_ids.T,
+        route_weights.T,
         (gate_weight[0], up_weight[0], down_weight[0]),
         (shared_gate, shared_up, shared_down),
         count,
         group,
     )
-    route_grad = jnp.sum(jnp.where(chosen, back_route.reshape(count, rows, 1), 0.0), axis=0)
+    token_grad, route_grad, gate_grad, up_grad, down_grad, shared_sum = flush(*held)
     return (
         token_grad,
-        route_grad,
+        route_grad.T,
         gate_grad[None],
         up_grad[None],
         down_grad[None],

time: 152 us -> 141 us (0.928)
  local copies, waits for them, and re-layouts: 9.54 us -> 0 us
  other arithmetic: 2.58 us -> 0 us
    unnamed x13 -> x0, local copies, waits for them, and re-layouts: 9.54 us -> none
    pallas_call x0 -> x1, Pallas kernels: none -> 2.93 us  [flush(): pl.pallas_call(functools.partial(flush_kernel, count), out_shape=tuple((j...]
    reduce_sum x2 -> x0, other arithmetic: 2.58 us -> none  [the longest x1 1.3 us: gathered_shards(): jnp.sum(jnp.where(chosen, route_weights[None], 0.0), axis=2)[:, None, :]]
    pallas_call x1, Pallas kernels: 139 us -> 137 us  [layer(): pl.pallas_call(functools.partial(layer_kernel, count, group), out_shape=(...]
where the time goes in v1:
time: 141 us
  Pallas kernels  140 us (99%)
    pallas_call x1, Pallas kernels, layer(): pl.pallas_call(functools.partial(layer_kernel, count, group), out_shape=(...  137 us
    pallas_call x1, Pallas kernels, flush(): pl.pallas_call(functools.partial(flush_kernel, count), out_shape=tuple((j...  2.93 us

profile of v1, /device:TPU:0, one launch (start us, length us, event | category | flops | bytes accessed | tf_op | source)
XLA Modules:
  0.0 140.5 jit_solution(12761213724775946363)
XLA Ops:
  0.6 137.0 %shard_map.145 = (bf16[128,2048]{1,0:T(8,128)(2,1)S(1)}, f32[4,128]{1,0:T(4,128)S(1)}, bf16[512,2048]{1,0:T(8,128)(2,1)S(1)}, bf16[512,2048]{1,0:T(8,128)(2,1)S(...) custom-call(bf16[128,2048]{1,0:T(8,128)(2,1)} %tok.1, bf16[128,2048]{1,0:T(8,128)(2,1)} %cot.1, ...), custom_call_target="tpu_custom_call" | custom-call | tf_op jit(solution)/shard_map/pallas_call | solution.py:488
  137.6 2.9 %shard_map.146 = (bf16[128,2048]{1,0:T(8,128)(2,1)}, f32[4,128]{1,0:T(4,128)}, bf16[512,2048]{1,0:T(8,128)(2,1)}, bf16[512,2048]{1,0:T(8,128)(2,1)}, bf16[512,2048]{1,0:T(8,128)(2,1)}, /*index=5*/f32[3,64,256]{2,1,0:T(8,128)}) custom-call(bf16[128,2048]{1,0:T(8,128)(2,1)S(1)} %get-tuple-element.18.refs_0_, f32[4,128]{1,0:T(4,128)S(1)} %get-tuple-element.19.refs_1_, ...), custom_call_target="tpu_custom_call" | custom-call | tf_op jit(solution)/shard_map/pallas_call | solution.py:551

commit v2 on v1

v2 whole, which is shorter than its diff:
```python
import functools

import jax
import jax.numpy as jnp
from jax import lax
from jax.experimental import pallas as pl
from jax.experimental.pallas import tpu as pltpu
from jax.sharding import PartitionSpec as P


def gated_backward(scaled, gate_pre, up_pre):
    sigmoid_gate = jax.nn.sigmoid(gate_pre)
    gate_delta = (scaled * up_pre * sigmoid_gate * (1.0 + gate_pre * (1.0 - sigmoid_gate))).astype(
        jnp.bfloat16
    )
    up_delta = (scaled * jax.nn.silu(gate_pre)).astype(jnp.bfloat16)
    return (gate_delta, up_delta)


def forward_products(token_rows, gate_local, up_local):
    gate_pre = jnp.einsum("rd,fd->rf", token_rows, gate_local, preferred_element_type=jnp.float32)
    up_pre = jnp.einsum("rd,fd->rf", token_rows, up_local, preferred_element_type=jnp.float32)
    return (gate_pre, up_pre)


def exchanged_shards(
    tokens,
    expert_ids,
    route_weights,
    cotangent,
    gate_weight,
    up_weight,
    down_weight,
    shared_gate,
    shared_up,
    shared_down,
):
    ep_size = lax.axis_size("ep")
    tok_rows = tokens.shape[0]
    model_width = tokens.shape[1]
    top_count = expert_ids.shape[1]
    capacity = 3 * tok_rows * top_count // (2 * ep_size)
    slots_all = ep_size * capacity
    assign_count = tok_rows * top_count
    flat_ids = expert_ids.reshape(-1)
    one_hot = (flat_ids[:, None] == jnp.arange(ep_size, dtype=jnp.int32)[None, :]).astype(jnp.int32)
    slot_index = jnp.sum(jnp.cumsum(one_hot, axis=0) * one_hot, axis=1) - 1
    position = flat_ids * capacity + slot_index
    row_assign = (
        jnp.full((slots_all,), assign_count, jnp.int32)
        .at[position]
        .set(jnp.arange(assign_count, dtype=jnp.int32))
    )
    row_token = row_assign // top_count
    row_weight = jnp.take(
        jnp.concatenate([route_weights.reshape(-1), jnp.zeros((1,), jnp.float32)], axis=0),
        row_assign,
        axis=0,
    )
    empty_row = jnp.zeros((1, model_width), jnp.bfloat16)
    send_tokens = jnp.take(jnp.concatenate([tokens, empty_row], axis=0), row_token, axis=0).reshape(
        ep_size, capacity, model_width
    )
    send_cot = jnp.take(jnp.concatenate([cotangent, empty_row], axis=0), row_token, axis=0).reshape(
        ep_size, capacity, model_width
    )
    gate_local = gate_weight[0]
    up_local = up_weight[0]
    down_local = down_weight[0]
    scales = lax.all_to_all(
        row_weight.reshape(ep_size, capacity), "ep", split_axis=0, concat_axis=0, tiled=True
    ).reshape(slots_all)
    token_rows, cot_rows = (
        lax.all_to_all(send_tokens, "ep", split_axis=0, concat_axis=0, tiled=True),
        lax.all_to_all(send_cot, "ep", split_axis=0, concat_axis=0, tiled=True),
    )
    token_rows = token_rows.reshape(slots_all, model_width)
    cot_rows = cot_rows.reshape(slots_all, model_width)
    gate_pre, up_pre = forward_products(token_rows, gate_local, up_local)
    hidden = (jax.nn.silu(gate_pre) * up_pre).astype(jnp.bfloat16)
    back_hidden = jnp.einsum("rd,fd->rf", cot_rows, down_local, preferred_element_type=jnp.float32)
    route_part = jnp.sum(back_hidden * hidden.astype(jnp.float32), axis=1)
    gate_delta, up_delta = gated_backward(scales[:, None] * back_hidden, gate_pre, up_pre)
    weighted_cot = (scales[:, None] * cot_rows.astype(jnp.float32)).astype(jnp.bfloat16)
    token_part = jnp.einsum(
        "rf,fd->rd", gate_delta, gate_local, preferred_element_type=jnp.float32
    ) + jnp.einsum("rf,fd->rd", up_delta, up_local, preferred_element_type=jnp.float32)
    gate_grad = jnp.einsum(
        "rf,rd->fd", gate_delta, token_rows, preferred_element_type=jnp.float32
    ).astype(jnp.bfloat16)[None]
    up_grad = jnp.einsum(
        "rf,rd->fd", up_delta, token_rows, preferred_element_type=jnp.float32
    ).astype(jnp.bfloat16)[None]
    down_grad = jnp.einsum(
        "rf,rd->fd", hidden, weighted_cot, preferred_element_type=jnp.float32
    ).astype(jnp.bfloat16)[None]
    back_rows, back_route = (
        lax.all_to_all(
            token_part.reshape(ep_size, capacity, model_width),
            "ep",
            split_axis=0,
            concat_axis=0,
            tiled=True,
        ),
        lax.all_to_all(
            route_part.reshape(ep_size, capacity), "ep", split_axis=0, concat_axis=0, tiled=True
        ),
    )
    routed = jnp.sum(
        jnp.take(back_rows.reshape(slots_all, model_width), position, axis=0).reshape(
            tok_rows, top_count, model_width
        ),
        axis=1,
    )
    route_grad = jnp.take(back_route.reshape(slots_all), position, axis=0).reshape(
        tok_rows, top_count
    )
    common_gate = jnp.einsum("td,fd->tf", tokens, shared_gate, preferred_element_type=jnp.float32)
    common_up = jnp.einsum("td,fd->tf", tokens, shared_up, preferred_element_type=jnp.float32)
    common_hidden = (jax.nn.silu(common_gate) * common_up).astype(jnp.bfloat16)
    common_back = jnp.einsum(
        "td,fd->tf", cotangent, shared_down, preferred_element_type=jnp.float32
    )
    common_gate_delta, common_up_delta = gated_backward(common_back, common_gate, common_up)
    common_part = jnp.einsum(
        "tf,fd->td", common_gate_delta, shared_gate, preferred_element_type=jnp.float32
    ) + jnp.einsum("tf,fd->td", common_up_delta, shared_up, preferred_element_type=jnp.float32)
    shared_grads = lax.psum_scatter(
        jnp.stack(
            [
                jnp.einsum(
                    "tc,tf->cf", tokens, common_gate_delta, preferred_element_type=jnp.float32
                ),
                jnp.einsum(
                    "tc,tf->cf", tokens, common_up_delta, preferred_element_type=jnp.float32
                ),
                jnp.einsum(
                    "tc,tf->cf", cotangent, common_hidden, preferred_element_type=jnp.float32
                ),
            ],
            axis=1,
        ),
        ("ep", "tp"),
        scatter_dimension=0,
        tiled=True,
    )
    token_grad = (routed + common_part).astype(jnp.bfloat16)
    return (token_grad, route_grad, gate_grad, up_grad, down_grad, shared_grads)


MESH = pl.DeviceIdType.MESH
LEVELS = 4
PIECES = 4


def greet(peers):
    barrier = pltpu.get_barrier_semaphore()
    for peer in peers:
        pl.semaphore_signal(barrier, inc=1, device_id=peer, device_id_type=MESH)
    pl.semaphore_wait(barrier, len(peers))


def remote(src, dst, send_sem, recv_sem, device):
    return pltpu.make_async_remote_copy(
        src_ref=src,
        dst_ref=dst,
        send_sem=send_sem,
        recv_sem=recv_sem,
        device_id=device,
        device_id_type=MESH,
    )


def dot_nt(left, right):
    return lax.dot_general(
        left, right, (((1,), (1,)), ((), ())), preferred_element_type=jnp.float32
    )


def dot(left, right):
    return jnp.dot(left, right, preferred_element_type=jnp.float32)


def deltas(scaled, gate_pre, up_pre):
    sigmoid_gate = jax.nn.sigmoid(gate_pre)
    silu_gate = gate_pre * sigmoid_gate
    gate_delta = scaled * up_pre * sigmoid_gate * (1.0 + gate_pre * (1.0 - sigmoid_gate))
    return gate_delta, scaled * silu_gate, silu_gate * up_pre


def layer_kernel(
    count,
    group,
    cap,
    tok,
    cot,
    ids,
    chosen_w,
    gate_w,
    up_w,
    down_w,
    shared_gate,
    shared_up,
    shared_down,
    token_out,
    route_out,
    gate_out,
    up_out,
    down_out,
    shared_out,
    meta,
    all_meta,
    route_buf,
    route_in,
    tok_w,
    cot_w,
    col,
    cmp_send,
    cmp_in,
    pre,
    turned,
    shared_turned,
    own_sum,
    other_sum,
    sum_send,
    sum_in,
    other_send,
    other_in,
    cross_send,
    cross_in,
    back_send,
    back_in,
    shared_part,
    shared_send,
    shared_in,
    load_sem,
    msend,
    mrecv,
    rsend,
    rrecv,
    zsend,
    zrecv,
    xsend,
    xrecv,
    dsend,
    drecv,
    osend,
    orecv,
    qsend,
    qrecv,
    bsend,
    brecv,
    ssend,
    srecv,
    own_sem,
):
    me = lax.axis_index("ep")
    mine = lax.axis_index("tp")
    level, side = lax.div(me, 2), lax.rem(me, 2)
    low = 1 - lax.div(level, LEVELS // 2)
    role = low * level + (1 - low) * (LEVELS - 1 - level)
    is_end, is_mid = role == 0, role == 1
    inner = {"ep": me + 4 * low - 2}
    outer = {"ep": me - 4 * low + 2}
    partner = {"ep": me + 1 - 2 * side}
    rows, width = tok.shape
    hid = gate_w.shape[0]
    common = shared_gate.shape[0]
    cut = width // PIECES
    every = tuple(range(PIECES))
    first, second = every[: PIECES // 2], every[PIECES // 2 :]

    def block_of(lev, column):
        return 2 * (low * lev + (1 - low) * (LEVELS - 1 - lev)) + column

    def piece(h):
        return pl.ds(h * cut, cut)

    loads = [
        pltpu.make_async_copy(src, dst, load_sem.at[i])
        for i, (src, dst) in enumerate(
            (
                (tok, col.at[0, role]),
                (cot, col.at[1, role]),
                (gate_w, tok_w.at[pl.ds(0, hid)]),
                (up_w, tok_w.at[pl.ds(hid, hid)]),
                (shared_gate, tok_w.at[pl.ds(2 * hid, common)]),
                (shared_up, tok_w.at[pl.ds(2 * hid + common, common)]),
                (down_w, cot_w.at[pl.ds(0, hid)]),
                (shared_down, cot_w.at[pl.ds(hid, common)]),
            )
        )
    ]
    for copy in loads:
        copy.start()

    lane = lax.broadcasted_iota(jnp.int32, (rows, rows), 1)
    depth = lax.broadcasted_iota(jnp.int32, (rows, rows), 0)
    before = jnp.where(depth <= lane, 1.0, 0.0).astype(jnp.bfloat16)
    for expert in range(count):
        named = ids[...] == expert
        meta[expert, 0] = jnp.sum(jnp.where(named, chosen_w[...], 0.0), axis=0, keepdims=True)
        hit = jnp.sum(jnp.where(named, 1.0, 0.0), axis=0, keepdims=True)
        place = dot(jnp.broadcast_to(hit, (8, rows)).astype(jnp.bfloat16), before)[:1]
        meta[expert, 1] = jnp.where(hit > 0.0, place - 1.0, -1.0)

    peers = [{"ep": lax.rem(me + step, count)} for step in range(1, count)]
    near = []
    for turn in range(2):
        for step in range(group):
            if turn + step > 0:
                near.append((turn, step, lax.rem(side + turn, 2), lax.rem(mine + step, group)))
    greet(
        peers
        + [
            {"ep": 2 * level + to_side, "tp": to_group}
            for turn, step, to_side, to_group in near
            if step > 0
        ]
    )

    def passed(array, lev, h, inward):
        if inward:
            lands = is_end * lev + is_mid * (LEVELS - 1 - lev)
        else:
            lands = lev
        return remote(
            col.at[array, lev, :, piece(h)],
            col.at[array, lands, :, piece(h)],
            zsend.at[1 - inward, array, lev, h],
            zrecv.at[array, lands, h],
            inner if inward else outer,
        )

    def arrival(array, lev, h):
        here = col.at[array, lev, :, piece(h)]
        return remote(here, here, zsend.at[0, array, lev, h], zrecv.at[array, lev, h], inner)

    def crossed(array, lev, h):
        return remote(
            cmp_send.at[array, lev, :, piece(h)],
            cmp_in.at[array, lev, pl.ds(0, cap), piece(h)],
            xsend.at[array, lev, h],
            xrecv.at[array, lev, h],
            partner,
        )

    def summed(lev, h):
        inward = lev > 0
        lands = is_end * lev + is_mid * (LEVELS - 1 - lev) if inward else lev
        return remote(
            sum_send.at[lev, :, piece(h)],
            sum_in.at[role, lands, :, piece(h)],
            dsend.at[lev, h],
            drecv.at[role, lands, h],
            inner if inward else outer,
        )

    def sum_wait(source, lev, h):
        remote(
            sum_send.at[lev, :, piece(h)],
            sum_in.at[source, lev, :, piece(h)],
            dsend.at[lev, h],
            drecv.at[source, lev, h],
            inner,
        ).wait_recv()

    def othered(lev, h):
        inward = lev > 0
        lands = is_end * lev + is_mid * (LEVELS - 1 - lev) if inward else lev
        return remote(
            other_send.at[lev, :, piece(h)],
            other_in.at[lands, :, piece(h)],
            osend.at[lev, h],
            orecv.at[lands, h],
            inner if inward else outer,
        )

    def other_wait(lev, h):
        remote(
            other_send.at[lev, :, piece(h)],
            other_in.at[lev, :, piece(h)],
            osend.at[lev, h],
            orecv.at[lev, h],
            inner,
        ).wait_recv()

    def over(h):
        return remote(
            cross_send.at[:, piece(h)],
            cross_in.at[:, piece(h)],
            qsend.at[h],
            qrecv.at[h],
            partner,
        )

    def returned(h):
        return remote(
            back_send.at[:, piece(h)],
            back_in.at[pl.ds(0, cap), piece(h)],
            bsend.at[h],
            brecv.at[h],
            partner,
        )

    def column_of(row):
        return jnp.sum(jnp.where(depth == lane, row, 0.0), axis=1, keepdims=True)

    def picks(row):
        return depth.astype(jnp.float32) == row

    def send_compact(array, lev, pieces):
        row = all_meta[block_of(lev, side), 1 - side, 1]
        chosen = jnp.where(picks(row), 1.0, 0.0).astype(jnp.bfloat16)[:cap]
        for h in pieces:
            cmp_send[array, lev, :, piece(h)] = dot(chosen, col[array, lev, :, piece(h)]).astype(
                jnp.bfloat16
            )
            crossed(array, lev, h).start()

    def arrive(array, lev, pieces):
        for h in pieces:
            arrival(array, lev, h).wait_recv()
            if isinstance(lev, int):
                if lev == 0:
                    passed(array, lev, h, 1).start()
                else:

                    @pl.when(is_mid)
                    def _():
                        passed(array, lev, h, 0).start()

            else:

                @pl.when(is_mid)
                def _():
                    passed(array, 0, h, 1).start()

            send_compact(array, lev, (h,))

    def send_sum(lev, pieces, source):
        for h in pieces:
            total = own_sum[lev, :, piece(h)]
            if lev == 2:
                row = all_meta[block_of(lev, side), 1 - side, 1]
                spread = jnp.where(
                    lane.astype(jnp.float32) == column_of(row), 1.0, 0.0
                ).astype(jnp.bfloat16)
                returned(h).wait_recv()
                total = total + dot(spread, back_in[:, piece(h)])
            if source is not None:
                sum_wait(source, lev, h)
                total = total + sum_in[source, lev, :, piece(h)].astype(jnp.float32)
            sum_send[lev, :, piece(h)] = total.astype(jnp.bfloat16)
            summed(lev, h).start()

    def send_other(lev, pieces, add):
        for h in pieces:
            total = other_sum[lev, :, piece(h)]
            if add:
                other_wait(lev, h)
                total = total + other_in[lev, :, piece(h)].astype(jnp.float32)
            other_send[lev, :, piece(h)] = total.astype(jnp.bfloat16)
            othered(lev, h).start()

    def send_over(pieces):
        for h in pieces:
            other_wait(role, h)
            total = other_sum[role, :, piece(h)] + other_in[role, :, piece(h)].astype(jnp.float32)
            cross_send[:, piece(h)] = total.astype(jnp.bfloat16)
            over(h).start()

    loads[0].wait()
    for h in every:
        passed(0, role, h, 1).start()

    @pl.when(is_mid)
    def _():
        for h in every:
            passed(0, 1, h, 0).start()

    loads[1].wait()

    @pl.when(is_end)
    def _():
        for h in every:
            passed(1, 0, h, 1).start()

    @pl.when(is_mid)
    def _():
        for h in every:
            passed(1, 1, h, 0).start()

    metas = []
    for step in range(1, count):
        peer = lax.rem(me + step, count)
        metas.append(
            remote(
                meta.at[pl.ds(2 * lax.div(peer, 2), 2)],
                all_meta.at[me],
                msend.at[step - 1],
                mrecv.at[step - 1],
                {"ep": peer},
            )
        )
    for copy in metas:
        copy.start()
    all_meta[me] = meta[pl.ds(2 * level, 2)]
    for array in (0, 1):
        send_compact(array, role, every)
    cmp_in[:, :, cap:] = jnp.zeros((2, LEVELS, rows - cap, width), jnp.bfloat16)
    back_in[cap:] = jnp.zeros((rows - cap, width), jnp.bfloat16)
    for copy in loads[2:]:
        copy.wait()
    for copy in metas:
        copy.wait()

    def full(lev, head):
        block = block_of(lev, side)
        same = depth == lane
        scale = column_of(all_meta[block, side, 0])
        pre[...] = dot_nt(col[0, lev], tok_w[...])
        back_hidden = dot_nt(col[1, lev], cot_w[pl.ds(0, hid)])
        gate_pre, up_pre = pre[:, pl.ds(0, hid)], pre[:, pl.ds(hid, hid)]
        gate_delta, up_delta, hidden = deltas(scale * back_hidden, gate_pre, up_pre)
        both = jnp.concatenate([gate_delta, up_delta], axis=1).astype(jnp.bfloat16)
        own_sum[lev] = dot(both, tok_w[pl.ds(0, 2 * hid)])
        rounded = hidden.astype(jnp.bfloat16).astype(jnp.float32)
        route = jnp.sum(back_hidden * rounded, axis=1, keepdims=True)
        route_buf[block] = jnp.sum(jnp.where(same, route, 0.0), axis=0, keepdims=True)
        columns = pl.ds(pl.multiple_of(lev * rows, rows), rows)
        turned[0, :, columns] = gate_delta.T.astype(jnp.bfloat16)
        turned[1, :, columns] = up_delta.T.astype(jnp.bfloat16)
        turned[2, :, columns] = (scale * hidden).T.astype(jnp.bfloat16)
        common_back = dot_nt(col[1, lev], cot_w[pl.ds(hid, common)])
        common_gate = pre[:, pl.ds(2 * hid, common)]
        common_up = pre[:, pl.ds(2 * hid + common, common)]
        common_deltas = deltas(common_back, common_gate, common_up)
        for i in range(3):
            shared_turned[i, :, columns] = common_deltas[i].T.astype(jnp.bfloat16)

        @pl.when(head)
        def _():
            pair = jnp.concatenate(common_deltas[:2], axis=1).astype(jnp.bfloat16)
            own_sum[lev] = own_sum[lev] + dot(pair, tok_w[pl.ds(2 * hid, 2 * common)])

    def compact(lev, last):
        for array in (0, 1):
            for h in every:
                crossed(array, lev, h).wait_recv()
        block = block_of(lev, 1 - side)
        weight_row, row = all_meta[block, side, 0], all_meta[block, side, 1]
        chosen = picks(row)
        scale = jnp.sum(jnp.where(chosen, weight_row, 0.0), axis=1, keepdims=True)
        pre[:, pl.ds(0, 2 * hid)] = dot_nt(cmp_in[0, lev], tok_w[pl.ds(0, 2 * hid)])
        back_hidden = dot_nt(cmp_in[1, lev], cot_w[pl.ds(0, hid)])
        gate_pre, up_pre = pre[:, pl.ds(0, hid)], pre[:, pl.ds(hid, hid)]
        gate_delta, up_delta, hidden = deltas(scale * back_hidden, gate_pre, up_pre)
        both = jnp.concatenate([gate_delta, up_delta], axis=1).astype(jnp.bfloat16)
        target = jnp.where(last, depth.astype(jnp.float32)[:, :1], column_of(row))
        spread = jnp.where(lane.astype(jnp.float32) == target, 1.0, 0.0).astype(jnp.bfloat16)
        other_sum[lev] = dot(
            dot(spread, both).astype(jnp.bfloat16), tok_w[pl.ds(0, 2 * hid)]
        )
        rounded = hidden.astype(jnp.bfloat16).astype(jnp.float32)
        route = jnp.sum(back_hidden * rounded, axis=1, keepdims=True)
        route_buf[block] = jnp.sum(jnp.where(chosen, route, 0.0), axis=0, keepdims=True)
        columns = pl.ds(pl.multiple_of((LEVELS + lev) * rows, rows), rows)
        turned[0, :, columns] = gate_delta.T.astype(jnp.bfloat16)
        turned[1, :, columns] = up_delta.T.astype(jnp.bfloat16)
        turned[2, :, columns] = (scale * hidden).T.astype(jnp.bfloat16)

    def body(i, carry):
        late = lax.div(i, 2)
        lev = (1 - late) * (i + role - 2 * i * role) + late * (5 - i)
        other_near = 1 - role

        @pl.when(i == 1)
        def _():
            arrive(1, other_near, second)

            @pl.when(is_mid)
            def _():
                for h in every:
                    passed(1, 1, h, 1).start()
                arrive(0, 3, second)

        @pl.when((i == 2) & is_end)
        def _():
            send_other(1, every, False)
            arrive(1, 3, every)

        @pl.when((i == 2) & is_mid)
        def _():
            arrive(1, 2, first)

        @pl.when((i == 3) & is_end)
        def _():
            send_other(3, every, False)
            arrive(0, 2, second)
            arrive(1, 2, every)

        @pl.when((i == 3) & is_mid)
        def _():
            send_over(second)

        full(lev, i == 0)

        @pl.when(i == 0)
        def _():
            arrive(0, other_near, every)
            arrive(1, other_near, first)

            @pl.when(is_mid)
            def _():
                arrive(0, 3, first)

        @pl.when((i == 1) & is_end)
        def _():
            send_sum(1, every, None)
            arrive(0, 3, every)

        @pl.when((i == 1) & is_mid)
        def _():
            arrive(1, 3, every)
            arrive(0, 2, every)

        @pl.when((i == 2) & is_end)
        def _():
            send_sum(3, every, None)
            arrive(0, 2, first)

        @pl.when((i == 2) & is_mid)
        def _():
            arrive(1, 2, second)
            send_over(first)

        @pl.when((i == 3) & is_mid)
        def _():
            send_sum(3, every, 0)
            send_sum(0, first, 1)
            send_other(3, first, True)

        compact(lev, i == LEVELS - 1)
        return carry

    lax.fori_loop(0, LEVELS, body, 0)

    for h in every:
        back_send[:, piece(h)] = other_sum[2, pl.ds(0, cap), piece(h)].astype(jnp.bfloat16)
        returned(h).start()

    @pl.when(is_mid)
    def _():
        send_sum(0, second, 1)
        send_other(3, second, True)

    routes = []
    for step in range(1, count):
        peer = lax.rem(me + step, count)
        routes.append(
            remote(
                route_buf.at[peer],
                route_in.at[me],
                rsend.at[step - 1],
                rrecv.at[step - 1],
                {"ep": peer},
            )
        )
    for copy in routes:
        copy.start()
    route_in[me] = route_buf[me]

    tile = 2 * common
    outs = (gate_out, up_out, down_out)

    def weight_grad(i):
        array = i // 2

        def tile_body(j, carry):
            cols = pl.ds(pl.multiple_of(j * tile, tile), tile)
            reach = LEVELS * rows
            grad = dot(turned[i, :, pl.ds(0, reach)], col[array, :, :, cols].reshape(reach, tile))
            grad = grad + dot(
                turned[i, :, pl.ds(reach, reach)], cmp_in[array, :, :, cols].reshape(reach, tile)
            )
            outs[i][:, cols] = grad.astype(jnp.bfloat16)
            return carry

        lax.fori_loop(0, width // tile, tile_body, 0)

    span = width // LEVELS
    size = span // (2 * group)
    mine_cols = pl.ds(pl.multiple_of(level * span, span), span)
    for i in range(3):
        block = col[i // 2, :, :, mine_cols].reshape(LEVELS * rows, span)
        grad = dot(shared_turned[i], block).T
        for to_side in range(2):
            for to_group in range(group):
                at = (to_side * group + to_group) * size
                shared_part[to_side, to_group, i] = grad[at : at + size]
                shared_send[to_side, to_group, i] = grad[at : at + size].astype(jnp.bfloat16)
    shares = [
        remote(
            shared_send.at[to_side, to_group],
            shared_in.at[side, mine],
            ssend.at[turn, step],
            srecv.at[turn, step],
            {"ep": 2 * level + to_side, "tp": to_group},
        )
        for turn, step, to_side, to_group in near
    ]
    for copy in shares:
        copy.start()

    weight_grad(0)

    @pl.when(is_end)
    def _():
        send_sum(2, every, None)

    @pl.when(is_mid)
    def _():
        send_other(0, every, True)

    weight_grad(1)

    @pl.when(is_mid)
    def _():
        send_sum(2, every, 0)

    weight_grad(2)

    @pl.when(is_end)
    def _():
        send_over(every)

    for copy in routes:
        copy.wait()
    found = jnp.zeros(ids.shape, jnp.float32)
    for expert in range(count):
        found = jnp.where(ids[...] == expert, route_in[expert], found)
    route_out[...] = found
    for copy in shares:
        copy.wait()
    total = shared_part[side, mine]
    for turn, step, to_side, to_group in near:
        total = total + shared_in[to_side, to_group].astype(jnp.float32)
    shared_out[...] = total

    @pl.when(is_mid)
    def _():
        for h in every:
            sum_wait(0, 1, h)
            own_sum[1, :, piece(h)] = own_sum[1, :, piece(h)] + sum_in[0, 1, :, piece(h)].astype(
                jnp.float32
            )

    for h in every:
        sum_wait(1, role, h)
        total = own_sum[role, :, piece(h)] + sum_in[1, role, :, piece(h)].astype(jnp.float32)
        over(h).wait_recv()
        total = total + cross_in[:, piece(h)].astype(jnp.float32)
        token_out[:, piece(h)] = total.astype(jnp.bfloat16)

    def sent(*copies):
        for copy in copies:
            copy.wait_send()

    for h in every:
        sent(over(h), returned(h))
        for array in (0, 1):
            sent(passed(array, role, h, 1))
            for lev in range(LEVELS):
                sent(crossed(array, lev, h))

        @pl.when(is_end)
        def _():
            sent(summed(1, h), summed(2, h), summed(3, h), othered(1, h), othered(3, h))

        @pl.when(is_mid)
        def _():
            sent(summed(0, h), summed(2, h), summed(3, h), othered(0, h), othered(3, h))
            for array in (0, 1):
                sent(passed(array, 0, h, 1))
                for lev in (1, 2, 3):
                    sent(passed(array, lev, h, 0))


def layer(tokens, cotangent, ids, weights, experts, commons, count, group, cap):
    rows, width = tokens.shape
    hid, common = experts[0].shape[0], commons[0].shape[0]
    piece = width // count // group
    vmem = pl.BlockSpec(memory_space=pltpu.VMEM)
    anywhere = pl.BlockSpec(memory_space=pl.ANY)
    grad = pltpu.VMEM((hid, width), jnp.bfloat16)
    shared = (3, piece, common)
    bf16, f32, dma = jnp.bfloat16, jnp.float32, pltpu.SemaphoreType.DMA
    return pl.pallas_call(
        functools.partial(layer_kernel, count, group, cap),
        out_shape=(
            pltpu.VMEM((rows, width), bf16),
            pltpu.VMEM(ids.shape, f32),
            grad,
            grad,
            grad,
            pltpu.VMEM(shared, f32),
        ),
        in_specs=[anywhere, anywhere, vmem, vmem] + [anywhere] * 6,
        out_specs=(vmem,) * 6,
        scratch_shapes=[
            pltpu.VMEM((count, 2, 1, rows), f32),
            pltpu.VMEM((count, 2, 2, 1, rows), f32),
            pltpu.VMEM((count, 1, rows), f32),
            pltpu.VMEM((count, 1, rows), f32),
            pltpu.VMEM((2 * hid + 2 * common, width), bf16),
            pltpu.VMEM((hid + common, width), bf16),
            pltpu.VMEM((2, LEVELS, rows, width), bf16),
            pltpu.VMEM((2, LEVELS, cap, width), bf16),
            pltpu.VMEM((2, LEVELS, rows, width), bf16),
            pltpu.VMEM((rows, 2 * hid + 2 * common), f32),
            pltpu.VMEM((3, hid, 2 * LEVELS * rows), bf16),
            pltpu.VMEM((3, common, LEVELS * rows), bf16),
            pltpu.VMEM((LEVELS, rows, width), f32),
            pltpu.VMEM((LEVELS, rows, width), f32),
            pltpu.VMEM((LEVELS, rows, width), bf16),
            pltpu.VMEM((2, LEVELS, rows, width), bf16),
            pltpu.VMEM((LEVELS, rows, width), bf16),
            pltpu.VMEM((LEVELS, rows, width), bf16),
            pltpu.VMEM((rows, width), bf16),
            pltpu.VMEM((rows, width), bf16),
            pltpu.VMEM((cap, width), bf16),
            pltpu.VMEM((rows, width), bf16),
            pltpu.VMEM((2, group) + shared, f32),
            pltpu.VMEM((2, group) + shared, bf16),
            pltpu.VMEM((2, group) + shared, bf16),
            dma((8,)),
            dma((count - 1,)),
            dma((count - 1,)),
            dma((count - 1,)),
            dma((count - 1,)),
            dma((2, 2, LEVELS, PIECES)),
            dma((2, LEVELS, PIECES)),
            dma((2, LEVELS, PIECES)),
            dma((2, LEVELS, PIECES)),
            dma((LEVELS, PIECES)),
            dma((2, LEVELS, PIECES)),
            dma((LEVELS, PIECES)),
            dma((LEVELS, PIECES)),
            dma((PIECES,)),
            dma((PIECES,)),
            dma((PIECES,)),
            dma((PIECES,)),
            dma((2, group)),
            dma((2, group)),
            dma((2,)),
        ],
        compiler_params=pltpu.CompilerParams(
            collective_id=0, has_side_effects=True, vmem_limit_bytes=55 * 2**20
        ),
    )(tokens, cotangent, ids, weights, *experts, *commons)


def flush_kernel(count, *refs):
    copies = [
        pltpu.make_async_copy(refs[i], refs[count + i], refs[2 * count].at[i]) for i in range(count)
    ]
    for copy in copies:
        copy.start()
    for copy in copies:
        copy.wait()


def flush(*held):
    count = len(held)
    return pl.pallas_call(
        functools.partial(flush_kernel, count),
        out_shape=tuple(jax.ShapeDtypeStruct(x.shape, x.dtype) for x in held),
        in_specs=[pl.BlockSpec(memory_space=pltpu.VMEM)] * count,
        out_specs=(pl.BlockSpec(memory_space=pl.ANY),) * count,
        scratch_shapes=[pltpu.SemaphoreType.DMA((count,))],
        compiler_params=pltpu.CompilerParams(vmem_limit_bytes=2**20),
    )(*held)


def gathered_shards(
    tokens,
    expert_ids,
    route_weights,
    cotangent,
    gate_weight,
    up_weight,
    down_weight,
    shared_gate,
    shared_up,
    shared_down,
):
    count, group = lax.axis_size("ep"), lax.axis_size("tp")
    held = layer(
        tokens,
        cotangent,
        expert_ids.T,
        route_weights.T,
        (gate_weight[0], up_weight[0], down_weight[0]),
        (shared_gate, shared_up, shared_down),
        count,
        group,
        3 * tokens.shape[0] * expert_ids.shape[1] // (2 * count),
    )
    token_grad, route_grad, gate_grad, up_grad, down_grad, shared_sum = flush(*held)
    return (
        token_grad,
        route_grad.T,
        gate_grad[None],
        up_grad[None],
        down_grad[None],
        jnp.transpose(shared_sum, (1, 0, 2)),
    )


def shards(tokens, expert_ids, *rest):
    dense = 2 * LEVELS == lax.axis_size("ep") <= 2 * expert_ids.shape[1]
    return (gathered_shards if dense else exchanged_shards)(tokens, expert_ids, *rest)


def solution(mesh):
    in_specs = (
        P(("ep", "tp"), None),
        P(("ep", "tp"), None),
        P(("ep", "tp"), None),
        P(("ep", "tp"), None),
        P(("ep", "tp"), None, None),
        P(("ep", "tp"), None, None),
        P(("ep", "tp"), None, None),
        P(),
        P(),
        P(),
    )
    out_specs = (
        P(("ep", "tp"), None),
        P(("ep", "tp"), None),
        P(("ep", "tp"), None, None),
        P(("ep", "tp"), None, None),
        P(("ep", "tp"), None, None),
        P(("ep", "tp"), None, None),
    )
    return jax.shard_map(shards, mesh=mesh, in_specs=in_specs, out_specs=out_specs, check_vma=False)
```

time: 141 us -> 131 us (0.929)
  Pallas kernels: 140 us -> 130 us
    pallas_call x1, Pallas kernels: 137 us -> 127 us  [layer(): pl.pallas_call(functools.partial(layer_kernel, count, group, cap), out_sh...]
where the time goes in v2:
time: 131 us; the launch traced here: 130 us
  Pallas kernels  130 us (99%)
    pallas_call x1, Pallas kernels, layer(): pl.pallas_call(functools.partial(layer_kernel, count, group, cap), out_sh...  127 us
    pallas_call x1, Pallas kernels, flush(): pl.pallas_call(functools.partial(flush_kernel, count), out_shape=tuple((j...  2.93 us

profile of v2, /device:TPU:0, one launch (start us, length us, event | category | flops | bytes accessed | tf_op | source)
XLA Modules:
  0.0 130.4 jit_solution(1548444449802410021)
XLA Ops:
  0.6 126.9 %shard_map.145 = (bf16[128,2048]{1,0:T(8,128)(2,1)S(1)}, f32[4,128]{1,0:T(4,128)S(1)}, bf16[512,2048]{1,0:T(8,128)(2,1)S(1)}, bf16[512,2048]{1,0:T(8,128)(2,1)S(...) custom-call(bf16[128,2048]{1,0:T(8,128)(2,1)} %tok.1, bf16[128,2048]{1,0:T(8,128)(2,1)} %cot.1, ...), custom_call_target="tpu_custom_call" | custom-call | tf_op jit(solution)/shard_map/pallas_call | solution.py:799
  127.5 2.9 %shard_map.146 = (bf16[128,2048]{1,0:T(8,128)(2,1)}, f32[4,128]{1,0:T(4,128)}, bf16[512,2048]{1,0:T(8,128)(2,1)}, bf16[512,2048]{1,0:T(8,128)(2,1)}, bf16[512,2048]{1,0:T(8,128)(2,1)}, /*index=5*/f32[3,64,256]{2,1,0:T(8,128)}) custom-call(bf16[128,2048]{1,0:T(8,128)(2,1)S(1)} %get-tuple-element.18.refs_0_, f32[4,128]{1,0:T(4,128)S(1)} %get-tuple-element.19.refs_1_, ...), custom_call_target="tpu_custom_call" | custom-call | tf_op jit(solution)/shard_map/pallas_call | solution.py:876

commit v3 on v2

--- a/solution.py
+++ b/solution.py
@@ -157,7 +157,7 @@
     barrier = pltpu.get_barrier_semaphore()
     for peer in peers:
         pl.semaphore_signal(barrier, inc=1, device_id=peer, device_id_type=MESH)
-    pl.semaphore_wait(barrier, len(peers))
+    return lambda: pl.semaphore_wait(barrier, len(peers))
 
 
 def remote(src, dst, send_sem, recv_sem, device):
@@ -218,6 +218,7 @@
     cmp_send,
     cmp_in,
     pre,
+    pre_other,
     turned,
     shared_turned,
     own_sum,
@@ -233,6 +234,8 @@
     shared_part,
     shared_send,
     shared_in,
+    pair_send,
+    pair_in,
     load_sem,
     msend,
     mrecv,
@@ -276,6 +279,10 @@
     def piece(h):
         return pl.ds(h * cut, cut)
 
+    peers = [{"ep": lax.rem(me + step, count)} for step in range(1, count)]
+    near = [lax.rem(mine + step, group) for step in range(1, group)]
+    greeted = greet(peers + [{"tp": to_group} for to_group in near])
+
     loads = [
         pltpu.make_async_copy(src, dst, load_sem.at[i])
         for i, (src, dst) in enumerate(
@@ -291,7 +298,7 @@
             )
         )
     ]
-    for copy in loads:
+    for copy in loads[:2]:
         copy.start()
 
     lane = lax.broadcasted_iota(jnp.int32, (rows, rows), 1)
@@ -304,20 +311,7 @@
         place = dot(jnp.broadcast_to(hit, (8, rows)).astype(jnp.bfloat16), before)[:1]
         meta[expert, 1] = jnp.where(hit > 0.0, place - 1.0, -1.0)
 
-    peers = [{"ep": lax.rem(me + step, count)} for step in range(1, count)]
-    near = []
-    for turn in range(2):
-        for step in range(group):
-            if turn + step > 0:
-                near.append((turn, step, lax.rem(side + turn, 2), lax.rem(mine + step, group)))
-    greet(
-        peers
-        + [
-            {"ep": 2 * level + to_side, "tp": to_group}
-            for turn, step, to_side, to_group in near
-            if step > 0
-        ]
-    )
+    greeted()
 
     def passed(array, lev, h, inward):
         if inward:
@@ -491,6 +485,8 @@
         for h in every:
             passed(1, 1, h, 0).start()
 
+    for copy in loads[2:]:
+        copy.start()
     metas = []
     for step in range(1, count):
         peer = lax.rem(me + step, count)
@@ -510,16 +506,16 @@
         send_compact(array, role, every)
     cmp_in[:, :, cap:] = jnp.zeros((2, LEVELS, rows - cap, width), jnp.bfloat16)
     back_in[cap:] = jnp.zeros((rows - cap, width), jnp.bfloat16)
-    for copy in loads[2:]:
-        copy.wait()
     for copy in metas:
         copy.wait()
+
+    def full_start(lev):
+        pre[...] = dot_nt(col[0, lev], tok_w[...])
 
     def full(lev, head):
         block = block_of(lev, side)
         same = depth == lane
         scale = column_of(all_meta[block, side, 0])
-        pre[...] = dot_nt(col[0, lev], tok_w[...])
         back_hidden = dot_nt(col[1, lev], cot_w[pl.ds(0, hid)])
         gate_pre, up_pre = pre[:, pl.ds(0, hid)], pre[:, pl.ds(hid, hid)]
         gate_delta, up_delta, hidden = deltas(scale * back_hidden, gate_pre, up_pre)
@@ -544,24 +540,35 @@
             pair = jnp.concatenate(common_deltas[:2], axis=1).astype(jnp.bfloat16)
             own_sum[lev] = own_sum[lev] + dot(pair, tok_w[pl.ds(2 * hid, 2 * common)])
 
+    def compact_start(lev):
+        for h in every:
+            crossed(0, lev, h).wait_recv()
+        pre_other[...] = dot_nt(cmp_in[0, lev], tok_w[pl.ds(0, 2 * hid)])
+
     def compact(lev, last):
-        for array in (0, 1):
-            for h in every:
-                crossed(array, lev, h).wait_recv()
+        for h in every:
+            crossed(1, lev, h).wait_recv()
         block = block_of(lev, 1 - side)
         weight_row, row = all_meta[block, side, 0], all_meta[block, side, 1]
         chosen = picks(row)
         scale = jnp.sum(jnp.where(chosen, weight_row, 0.0), axis=1, keepdims=True)
-        pre[:, pl.ds(0, 2 * hid)] = dot_nt(cmp_in[0, lev], tok_w[pl.ds(0, 2 * hid)])
         back_hidden = dot_nt(cmp_in[1, lev], cot_w[pl.ds(0, hid)])
-        gate_pre, up_pre = pre[:, pl.ds(0, hid)], pre[:, pl.ds(hid, hid)]
+        gate_pre, up_pre = pre_other[:, pl.ds(0, hid)], pre_other[:, pl.ds(hid, hid)]
         gate_delta, up_delta, hidden = deltas(scale * back_hidden, gate_pre, up_pre)
         both = jnp.concatenate([gate_delta, up_delta], axis=1).astype(jnp.bfloat16)
         target = jnp.where(last, depth.astype(jnp.float32)[:, :1], column_of(row))
         spread = jnp.where(lane.astype(jnp.float32) == target, 1.0, 0.0).astype(jnp.bfloat16)
-        other_sum[lev] = dot(
-            dot(spread, both).astype(jnp.bfloat16), tok_w[pl.ds(0, 2 * hid)]
-        )
+        both = dot(spread, both).astype(jnp.bfloat16)
+        for h in every:
+            other_sum[lev, :, piece(h)] = dot(both, tok_w[pl.ds(0, 2 * hid), piece(h)])
+
+            @pl.when(last)
+            def _():
+                back_send[:, piece(h)] = other_sum[lev, pl.ds(0, cap), piece(h)].astype(
+                    jnp.bfloat16
+                )
+                returned(h).start()
+
         rounded = hidden.astype(jnp.bfloat16).astype(jnp.float32)
         route = jnp.sum(back_hidden * rounded, axis=1, keepdims=True)
         route_buf[block] = jnp.sum(jnp.where(chosen, route, 0.0), axis=0, keepdims=True)
@@ -575,9 +582,38 @@
         lev = (1 - late) * (i + role - 2 * i * role) + late * (5 - i)
         other_near = 1 - role
 
+        @pl.when((i == 2) & is_end)
+        def _():
+            send_other(1, every, False)
+
+        @pl.when((i == 3) & is_end)
+        def _():
+            send_other(3, every, False)
+            arrive(0, 2, second)
+
+        @pl.when((i == 3) & is_mid)
+        def _():
+            send_over(second)
+
+        @pl.when(i == 0)
+        def _():
+            arrive(0, other_near, first)
+            for copy in loads[2:]:
+                copy.wait()
+
         @pl.when(i == 1)
         def _():
-            arrive(1, other_near, second)
+            arrive(1, other_near, second[:1])
+
+        full_start(lev)
+
+        @pl.when(i == 0)
+        def _():
+            arrive(0, other_near, second)
+
+        @pl.when(i == 1)
+        def _():
+            arrive(1, other_near, second[1:])
 
             @pl.when(is_mid)
             def _():
@@ -587,7 +623,6 @@
 
         @pl.when((i == 2) & is_end)
         def _():
-            send_other(1, every, False)
             arrive(1, 3, every)
 
         @pl.when((i == 2) & is_mid)
@@ -596,20 +631,37 @@
 
         @pl.when((i == 3) & is_end)
         def _():
-            send_other(3, every, False)
-            arrive(0, 2, second)
             arrive(1, 2, every)
 
+        full(lev, i == 0)
+
+        @pl.when(i == 0)
+        def _():
+            arrive(1, other_near, first[:1])
+
+        @pl.when((i == 1) & is_end)
+        def _():
+            send_sum(1, every, None)
+
+        @pl.when((i == 2) & is_end)
+        def _():
+            send_sum(3, every, None)
+
+        @pl.when((i == 2) & is_mid)
+        def _():
+            arrive(1, 2, second)
+
         @pl.when((i == 3) & is_mid)
         def _():
-            send_over(second)
-
-        full(lev, i == 0)
+            send_sum(3, every, 0)
+            send_sum(0, first, 1)
+            send_other(3, first, True)
+
+        compact_start(lev)
 
         @pl.when(i == 0)
         def _():
-            arrive(0, other_near, every)
-            arrive(1, other_near, first)
+            arrive(1, other_near, first[1:])
 
             @pl.when(is_mid)
             def _():
@@ -617,7 +669,6 @@
 
         @pl.when((i == 1) & is_end)
         def _():
-            send_sum(1, every, None)
             arrive(0, 3, every)
 
         @pl.when((i == 1) & is_mid)
@@ -627,28 +678,16 @@
 
         @pl.when((i == 2) & is_end)
         def _():
-            send_sum(3, every, None)
             arrive(0, 2, first)
 
         @pl.when((i == 2) & is_mid)
         def _():
-            arrive(1, 2, second)
             send_over(first)
-
-        @pl.when((i == 3) & is_mid)
-        def _():
-            send_sum(3, every, 0)
-            send_sum(0, first, 1)
-            send_other(3, first, True)
 
         compact(lev, i == LEVELS - 1)
         return carry
 
     lax.fori_loop(0, LEVELS, body, 0)
-
-    for h in every:
-        back_send[:, piece(h)] = other_sum[2, pl.ds(0, cap), piece(h)].astype(jnp.bfloat16)
-        returned(h).start()
 
     @pl.when(is_mid)
     def _():
@@ -698,42 +737,54 @@
         for to_side in range(2):
             for to_group in range(group):
                 at = (to_side * group + to_group) * size
-                shared_part[to_side, to_group, i] = grad[at : at + size]
-                shared_send[to_side, to_group, i] = grad[at : at + size].astype(jnp.bfloat16)
+                shared_part[to_group, to_side, i] = grad[at : at + size]
+                shared_send[to_group, to_side, i] = grad[at : at + size].astype(jnp.bfloat16)
     shares = [
         remote(
-            shared_send.at[to_side, to_group],
-            shared_in.at[side, mine],
-            ssend.at[turn, step],
-            srecv.at[turn, step],
-            {"ep": 2 * level + to_side, "tp": to_group},
+            shared_send.at[to_group],
+            shared_in.at[mine],
+            ssend.at[step],
+            srecv.at[step],
+            {"tp": to_group},
         )
-        for turn, step, to_side, to_group in near
+        for step, to_group in enumerate(near)
     ]
     for copy in shares:
         copy.start()
 
-    weight_grad(0)
-
     @pl.when(is_end)
     def _():
         send_sum(2, every, None)
+        send_over(first)
 
     @pl.when(is_mid)
     def _():
         send_other(0, every, True)
 
-    weight_grad(1)
+    weight_grad(0)
+
+    @pl.when(is_end)
+    def _():
+        send_over(second)
 
     @pl.when(is_mid)
     def _():
         send_sum(2, every, 0)
 
+    weight_grad(1)
+
+    for copy in shares:
+        copy.wait()
+    for to_side in range(2):
+        total = shared_part[mine, to_side]
+        for to_group in near:
+            total = total + shared_in[to_group, to_side].astype(jnp.float32)
+        shared_part[mine, to_side] = total
+    pair_send[...] = shared_part[mine, 1 - side].astype(jnp.bfloat16)
+    pair = remote(pair_send, pair_in, ssend.at[group - 1], srecv.at[group - 1], partner)
+    pair.start()
+
     weight_grad(2)
-
-    @pl.when(is_end)
-    def _():
-        send_over(every)
 
     for copy in routes:
         copy.wait()
@@ -741,12 +792,8 @@
     for expert in range(count):
         found = jnp.where(ids[...] == expert, route_in[expert], found)
     route_out[...] = found
-    for copy in shares:
-        copy.wait()
-    total = shared_part[side, mine]
-    for turn, step, to_side, to_group in near:
-        total = total + shared_in[to_side, to_group].astype(jnp.float32)
-    shared_out[...] = total
+    pair.wait()
+    shared_out[...] = shared_part[mine, side] + pair_in[...].astype(jnp.float32)
 
     @pl.when(is_mid)
     def _():
@@ -819,6 +866,7 @@
             pltpu.VMEM((2, LEVELS, cap, width), bf16),
             pltpu.VMEM((2, LEVELS, rows, width), bf16),
             pltpu.VMEM((rows, 2 * hid + 2 * common), f32),
+            pltpu.VMEM((rows, 2 * hid), f32),
             pltpu.VMEM((3, hid, 2 * LEVELS * rows), bf16),
             pltpu.VMEM((3, common, LEVELS * rows), bf16),
             pltpu.VMEM((LEVELS, rows, width), f32),
@@ -831,9 +879,11 @@
             pltpu.VMEM((rows, width), bf16),
             pltpu.VMEM((cap, width), bf16),
             pltpu.VMEM((rows, width), bf16),
-            pltpu.VMEM((2, group) + shared, f32),
-            pltpu.VMEM((2, group) + shared, bf16),
-            pltpu.VMEM((2, group) + shared, bf16),
+            pltpu.VMEM((group, 2) + shared, f32),
+            pltpu.VMEM((group, 2) + shared, bf16),
+            pltpu.VMEM((group, 2) + shared, bf16),
+            pltpu.VMEM(shared, bf16),
+            pltpu.VMEM(shared, bf16),
             dma((8,)),
             dma((count - 1,)),
             dma((count - 1,)),
@@ -851,8 +901,8 @@
             dma((PIECES,)),
             dma((PIECES,)),
             dma((PIECES,)),
-            dma((2, group)),
-            dma((2, group)),
+            dma((group,)),
+            dma((group,)),
             dma((2,)),
         ],
         compiler_params=pltpu.CompilerParams(

time: 131 us -> 122 us (0.931)
  Pallas kernels: 130 us -> 121 us
    pallas_call x1, Pallas kernels: 127 us -> 118 us  [layer(): pl.pallas_call(functools.partial(layer_kernel, count, group, cap), out_sh...]
where the time goes in v3:
time: 122 us
  Pallas kernels  121 us (99%)
    pallas_call x1, Pallas kernels, layer(): pl.pallas_call(functools.partial(layer_kernel, count, group, cap), out_sh...  118 us
    pallas_call x1, Pallas kernels, flush(): pl.pallas_call(functools.partial(flush_kernel, count), out_shape=tuple((j...  2.93 us

profile of v3, /device:TPU:0, one launch (start us, length us, event | category | flops | bytes accessed | tf_op | source)
XLA Modules:
  0.0 121.8 jit_solution(13168085689036539266)
XLA Ops:
  0.6 118.2 %shard_map.145 = (bf16[128,2048]{1,0:T(8,128)(2,1)S(1)}, f32[4,128]{1,0:T(4,128)S(1)}, bf16[512,2048]{1,0:T(8,128)(2,1)S(1)}, bf16[512,2048]{1,0:T(8,128)(2,1)S(...) custom-call(bf16[128,2048]{1,0:T(8,128)(2,1)} %tok.1, bf16[128,2048]{1,0:T(8,128)(2,1)} %cot.1, ...), custom_call_target="tpu_custom_call" | custom-call | tf_op jit(solution)/shard_map/pallas_call | solution.py:846
  118.9 2.9 %shard_map.146 = (bf16[128,2048]{1,0:T(8,128)(2,1)}, f32[4,128]{1,0:T(4,128)}, bf16[512,2048]{1,0:T(8,128)(2,1)}, bf16[512,2048]{1,0:T(8,128)(2,1)}, bf16[512,2048]{1,0:T(8,128)(2,1)}, /*index=5*/f32[3,64,256]{2,1,0:T(8,128)}) custom-call(bf16[128,2048]{1,0:T(8,128)(2,1)S(1)} %get-tuple-element.18.refs_0_, f32[4,128]{1,0:T(4,128)S(1)} %get-tuple-element.19.refs_1_, ...), custom_call_target="tpu_custom_call" | custom-call | tf_op jit(solution)/shard_map/pallas_call | solution.py:926

commit v4 on v3

--- a/solution.py
+++ b/solution.py
@@ -194,8 +194,8 @@
     cap,
     tok,
     cot,
-    ids,
-    chosen_w,
+    ids_from,
+    chosen_from,
     gate_w,
     up_w,
     down_w,
@@ -208,6 +208,8 @@
     up_out,
     down_out,
     shared_out,
+    ids,
+    chosen_w,
     meta,
     all_meta,
     route_buf,
@@ -289,6 +291,8 @@
             (
                 (tok, col.at[0, role]),
                 (cot, col.at[1, role]),
+                (ids_from, ids),
+                (chosen_from, chosen_w),
                 (gate_w, tok_w.at[pl.ds(0, hid)]),
                 (up_w, tok_w.at[pl.ds(hid, hid)]),
                 (shared_gate, tok_w.at[pl.ds(2 * hid, common)]),
@@ -298,8 +302,10 @@
             )
         )
     ]
-    for copy in loads[:2]:
+    for copy in loads[2:4] + loads[:2]:
         copy.start()
+    for copy in loads[2:4]:
+        copy.wait()
 
     lane = lax.broadcasted_iota(jnp.int32, (rows, rows), 1)
     depth = lax.broadcasted_iota(jnp.int32, (rows, rows), 0)
@@ -433,13 +439,14 @@
             send_compact(array, lev, (h,))
 
     def send_sum(lev, pieces, source):
+        if lev == 2:
+            row = all_meta[block_of(lev, side), 1 - side, 1]
+            spread = jnp.where(
+                lane.astype(jnp.float32) == column_of(row), 1.0, 0.0
+            ).astype(jnp.bfloat16)
         for h in pieces:
             total = own_sum[lev, :, piece(h)]
             if lev == 2:
-                row = all_meta[block_of(lev, side), 1 - side, 1]
-                spread = jnp.where(
-                    lane.astype(jnp.float32) == column_of(row), 1.0, 0.0
-                ).astype(jnp.bfloat16)
                 returned(h).wait_recv()
                 total = total + dot(spread, back_in[:, piece(h)])
             if source is not None:
@@ -485,7 +492,7 @@
         for h in every:
             passed(1, 1, h, 0).start()
 
-    for copy in loads[2:]:
+    for copy in loads[4:]:
         copy.start()
     metas = []
     for step in range(1, count):
@@ -521,24 +528,28 @@
         gate_delta, up_delta, hidden = deltas(scale * back_hidden, gate_pre, up_pre)
         both = jnp.concatenate([gate_delta, up_delta], axis=1).astype(jnp.bfloat16)
         own_sum[lev] = dot(both, tok_w[pl.ds(0, 2 * hid)])
-        rounded = hidden.astype(jnp.bfloat16).astype(jnp.float32)
-        route = jnp.sum(back_hidden * rounded, axis=1, keepdims=True)
-        route_buf[block] = jnp.sum(jnp.where(same, route, 0.0), axis=0, keepdims=True)
-        columns = pl.ds(pl.multiple_of(lev * rows, rows), rows)
-        turned[0, :, columns] = gate_delta.T.astype(jnp.bfloat16)
-        turned[1, :, columns] = up_delta.T.astype(jnp.bfloat16)
-        turned[2, :, columns] = (scale * hidden).T.astype(jnp.bfloat16)
-        common_back = dot_nt(col[1, lev], cot_w[pl.ds(hid, common)])
-        common_gate = pre[:, pl.ds(2 * hid, common)]
-        common_up = pre[:, pl.ds(2 * hid + common, common)]
-        common_deltas = deltas(common_back, common_gate, common_up)
-        for i in range(3):
-            shared_turned[i, :, columns] = common_deltas[i].T.astype(jnp.bfloat16)
-
-        @pl.when(head)
-        def _():
-            pair = jnp.concatenate(common_deltas[:2], axis=1).astype(jnp.bfloat16)
-            own_sum[lev] = own_sum[lev] + dot(pair, tok_w[pl.ds(2 * hid, 2 * common)])
+
+        def rest():
+            rounded = hidden.astype(jnp.bfloat16).astype(jnp.float32)
+            route = jnp.sum(back_hidden * rounded, axis=1, keepdims=True)
+            route_buf[block] = jnp.sum(jnp.where(same, route, 0.0), axis=0, keepdims=True)
+            columns = pl.ds(pl.multiple_of(lev * rows, rows), rows)
+            turned[0, :, columns] = gate_delta.T.astype(jnp.bfloat16)
+            turned[1, :, columns] = up_delta.T.astype(jnp.bfloat16)
+            turned[2, :, columns] = (scale * hidden).T.astype(jnp.bfloat16)
+            common_back = dot_nt(col[1, lev], cot_w[pl.ds(hid, common)])
+            common_gate = pre[:, pl.ds(2 * hid, common)]
+            common_up = pre[:, pl.ds(2 * hid + common, common)]
+            common_deltas = deltas(common_back, common_gate, common_up)
+            for i in range(3):
+                shared_turned[i, :, columns] = common_deltas[i].T.astype(jnp.bfloat16)
+
+            @pl.when(head)
+            def _():
+                pair = jnp.concatenate(common_deltas[:2], axis=1).astype(jnp.bfloat16)
+                own_sum[lev] = own_sum[lev] + dot(pair, tok_w[pl.ds(2 * hid, 2 * common)])
+
+        return rest
 
     def compact_start(lev):
         for h in every:
@@ -569,26 +580,24 @@
                 )
                 returned(h).start()
 
-        rounded = hidden.astype(jnp.bfloat16).astype(jnp.float32)
-        route = jnp.sum(back_hidden * rounded, axis=1, keepdims=True)
-        route_buf[block] = jnp.sum(jnp.where(chosen, route, 0.0), axis=0, keepdims=True)
-        columns = pl.ds(pl.multiple_of((LEVELS + lev) * rows, rows), rows)
-        turned[0, :, columns] = gate_delta.T.astype(jnp.bfloat16)
-        turned[1, :, columns] = up_delta.T.astype(jnp.bfloat16)
-        turned[2, :, columns] = (scale * hidden).T.astype(jnp.bfloat16)
+        def rest():
+            rounded = hidden.astype(jnp.bfloat16).astype(jnp.float32)
+            route = jnp.sum(back_hidden * rounded, axis=1, keepdims=True)
+            route_buf[block] = jnp.sum(jnp.where(chosen, route, 0.0), axis=0, keepdims=True)
+            columns = pl.ds(pl.multiple_of((LEVELS + lev) * rows, rows), rows)
+            turned[0, :, columns] = gate_delta.T.astype(jnp.bfloat16)
+            turned[1, :, columns] = up_delta.T.astype(jnp.bfloat16)
+            turned[2, :, columns] = (scale * hidden).T.astype(jnp.bfloat16)
+
+        return rest
 
     def body(i, carry):
         late = lax.div(i, 2)
         lev = (1 - late) * (i + role - 2 * i * role) + late * (5 - i)
         other_near = 1 - role
 
-        @pl.when((i == 2) & is_end)
-        def _():
-            send_other(1, every, False)
-
         @pl.when((i == 3) & is_end)
         def _():
-            send_other(3, every, False)
             arrive(0, 2, second)
 
         @pl.when((i == 3) & is_mid)
@@ -598,7 +607,7 @@
         @pl.when(i == 0)
         def _():
             arrive(0, other_near, first)
-            for copy in loads[2:]:
+            for copy in loads[4:]:
                 copy.wait()
 
         @pl.when(i == 1)
@@ -633,27 +642,33 @@
         def _():
             arrive(1, 2, every)
 
-        full(lev, i == 0)
+        @pl.when((i == 3) & is_mid)
+        def _():
+            send_sum(3, first, 0)
+
+        rest = full(lev, i == 0)
+
+        @pl.when((i == 1) & is_end)
+        def _():
+            send_sum(1, every, None)
+
+        @pl.when((i == 2) & is_end)
+        def _():
+            send_sum(3, every, None)
+
+        rest()
 
         @pl.when(i == 0)
         def _():
             arrive(1, other_near, first[:1])
 
-        @pl.when((i == 1) & is_end)
-        def _():
-            send_sum(1, every, None)
-
-        @pl.when((i == 2) & is_end)
-        def _():
-            send_sum(3, every, None)
-
         @pl.when((i == 2) & is_mid)
         def _():
             arrive(1, 2, second)
 
         @pl.when((i == 3) & is_mid)
         def _():
-            send_sum(3, every, 0)
+            send_sum(3, second, 0)
             send_sum(0, first, 1)
             send_other(3, first, True)
 
@@ -684,7 +699,17 @@
         def _():
             send_over(first)
 
-        compact(lev, i == LEVELS - 1)
+        rest = compact(lev, i == LEVELS - 1)
+
+        @pl.when((i == 1) & is_end)
+        def _():
+            send_other(1, every, False)
+
+        @pl.when((i == 2) & is_end)
+        def _():
+            send_other(3, every, False)
+
+        rest()
         return carry
 
     lax.fori_loop(0, LEVELS, body, 0)
@@ -752,6 +777,12 @@
     for copy in shares:
         copy.start()
 
+    @pl.when(is_mid)
+    def _():
+        send_other(0, every, True)
+
+    weight_grad(0)
+
     @pl.when(is_end)
     def _():
         send_sum(2, every, None)
@@ -759,19 +790,21 @@
 
     @pl.when(is_mid)
     def _():
-        send_other(0, every, True)
-
-    weight_grad(0)
+        send_sum(2, every, 0)
+
+    @pl.when(is_mid)
+    def _():
+        for h in every:
+            sum_wait(0, 1, h)
+            own_sum[1, :, piece(h)] = own_sum[1, :, piece(h)] + sum_in[0, 1, :, piece(h)].astype(
+                jnp.float32
+            )
+
+    weight_grad(1)
 
     @pl.when(is_end)
     def _():
         send_over(second)
-
-    @pl.when(is_mid)
-    def _():
-        send_sum(2, every, 0)
-
-    weight_grad(1)
 
     for copy in shares:
         copy.wait()
@@ -794,14 +827,6 @@
     route_out[...] = found
     pair.wait()
     shared_out[...] = shared_part[mine, side] + pair_in[...].astype(jnp.float32)
-
-    @pl.when(is_mid)
-    def _():
-        for h in every:
-            sum_wait(0, 1, h)
-            own_sum[1, :, piece(h)] = own_sum[1, :, piece(h)] + sum_in[0, 1, :, piece(h)].astype(
-                jnp.float32
-            )
 
     for h in every:
         sum_wait(1, role, h)
@@ -853,9 +878,11 @@
             grad,
             pltpu.VMEM(shared, f32),
         ),
-        in_specs=[anywhere, anywhere, vmem, vmem] + [anywhere] * 6,
+        in_specs=[anywhere] * 10,
         out_specs=(vmem,) * 6,
         scratch_shapes=[
+            pltpu.VMEM(ids.shape, ids.dtype),
+            pltpu.VMEM(weights.shape, weights.dtype),
             pltpu.VMEM((count, 2, 1, rows), f32),
             pltpu.VMEM((count, 2, 2, 1, rows), f32),
             pltpu.VMEM((count, 1, rows), f32),
@@ -884,7 +911,7 @@
             pltpu.VMEM((group, 2) + shared, bf16),
             pltpu.VMEM(shared, bf16),
             pltpu.VMEM(shared, bf16),
-            dma((8,)),
+            dma((10,)),
             dma((count - 1,)),
             dma((count - 1,)),
             dma((count - 1,)),

time: 122 us -> 121 us (level)
  no operation moved by 1% of the time
where the time goes in v4:
time: 121 us
  Pallas kernels  120 us (99%)
    pallas_call x1, Pallas kernels, layer(): pl.pallas_call(functools.partial(layer_kernel, count, group, cap), out_sh...  117 us
    pallas_call x1, Pallas kernels, flush(): pl.pallas_call(functools.partial(flush_kernel, count), out_shape=tuple((j...  2.93 us

profile of v4, /device:TPU:0, one launch (start us, length us, event | category | flops | bytes accessed | tf_op | source)
XLA Modules:
  0.0 120.8 jit_solution(12470354520693726366)
XLA Ops:
  0.6 117.2 %shard_map.145 = (bf16[128,2048]{1,0:T(8,128)(2,1)S(1)}, f32[4,128]{1,0:T(4,128)S(1)}, bf16[512,2048]{1,0:T(8,128)(2,1)S(1)}, bf16[512,2048]{1,0:T(8,128)(2,1)S(...) custom-call(bf16[128,2048]{1,0:T(8,128)(2,1)} %tok.1, bf16[128,2048]{1,0:T(8,128)(2,1)} %cot.1, ...), custom_call_target="tpu_custom_call" | custom-call | tf_op jit(solution)/shard_map/pallas_call | solution.py:871
  117.9 2.9 %shard_map.146 = (bf16[128,2048]{1,0:T(8,128)(2,1)}, f32[4,128]{1,0:T(4,128)}, bf16[512,2048]{1,0:T(8,128)(2,1)}, bf16[512,2048]{1,0:T(8,128)(2,1)}, bf16[512,2048]{1,0:T(8,128)(2,1)}, /*index=5*/f32[3,64,256]{2,1,0:T(8,128)}) custom-call(bf16[128,2048]{1,0:T(8,128)(2,1)S(1)} %get-tuple-element.18.refs_0_, f32[4,128]{1,0:T(4,128)S(1)} %get-tuple-element.19.refs_1_, ...), custom_call_target="tpu_custom_call" | custom-call | tf_op jit(solution)/shard_map/pallas_call | solution.py:953
